TPU v7x, 256 devices: a 4x2x16 block of a 4x16x16 slice. The times are simulated.
256 devices in a mesh: grp: 2 (over y), ep: 64 (over z, x), tp: 2 (over core).
Axes of the slice: x: 4, y: 2, z: 16, core: 2. Of those that a mesh axis runs over, the one named last changes fastest.
The devices are a block of a 4x16x16 slice.
Arguments:
- tokens: bfloat16 [65536, 2048], P(('grp', 'ep', 'tp')), parts along dimension 0, may hold values from -15 to 15
- gain_in: float32 [2048], replicated, may hold values from 0.1 to 1.9
- expert_ids: int32 [65536, 2], P(('grp', 'ep')), parts along dimension 0, may hold values from 0 to 63, all different within a row; in each aligned block of 256 rows (0 to 255, 256 to 511, ...) at most 16 rows name the same one
- gate_weights: float32 [65536, 2], P(('grp', 'ep')), parts along dimension 0, may hold values from 0.1 to 1
- w_gate: bfloat16 [64, 2048, 512], P('ep', None, 'tp'), may hold values from -0.125 to 0.125
- w_up: bfloat16 [64, 2048, 512], P('ep', None, 'tp'), may hold values from -0.125 to 0.125
- w_down: bfloat16 [64, 2048, 512], P('ep', None, 'tp'), may hold values from -20 to 20
- gain_out: float32 [2048], P('tp'), may hold values from 0.1 to 1.9
Outputs:
- mixed: bfloat16 [65536, 2048], P(('grp', 'ep'), 'tp'), parts along dimension 0
There are 2 independent parts, one for each index of `grp`. A program takes and returns all parts, laid end to end along the dimension named above; an argument that names none is the same for every part. Nothing has to cross between parts.
Inputs may be any that keep to these rules, and one draw needn't show every extreme that they name: `expert_ids`: each token names 2 different experts; in each aligned block of 256 tokens no expert is named by more than 16 pairs, a bound that some block reaches.
All inputs are finite; a program needn't handle non-finite values.
Results may differ from a plain program's by a relative error of at most 0.0077.
Values may be sent and summed in bfloat16 or wider, within the bound.
A program may use at most 64 MiB of HBM per device.

v0:
```python
import jax
import jax.numpy as jnp
from jax import lax
from jax.sharding import PartitionSpec as P

EPS = 1e-06


def side_by_side(arrays, axis, dim, along):
    widths = [a.shape[along] for a in arrays]
    both = jnp.concatenate(arrays, axis=along)
    filled = lax.all_gather(both, axis, axis=dim, tiled=True)
    return tuple(jnp.split(filled, [sum(widths[:k]) for k in range(1, len(widths))], axis=along))


def block_slots(expert_ids, block_rows, experts):
    pairs = expert_ids.reshape(-1, block_rows * expert_ids.shape[1])
    onehot = (pairs[:, :, None] == jnp.arange(experts, dtype=jnp.int32)[None, None, :]).astype(
        jnp.int32
    )
    before = jnp.cumsum(onehot, axis=1) - onehot
    return jnp.sum(before * onehot, axis=2).reshape(expert_ids.shape)


def swiglu_rows(rows, gate_matrix, up_matrix):
    flat = rows.reshape(-1, rows.shape[-1])
    gated = jnp.dot(flat, gate_matrix, preferred_element_type=jnp.float32)
    upward = jnp.dot(flat, up_matrix, preferred_element_type=jnp.float32)
    hidden = (jax.nn.silu(gated) * upward).astype(jnp.bfloat16)
    return hidden.reshape(rows.shape[:-1] + (gate_matrix.shape[1],))


def down_block(hidden, down_matrix):
    return lax.dot_general(
        hidden,
        down_matrix,
        (((hidden.ndim - 1,), (1,)), ((), ())),
        preferred_element_type=jnp.float32,
    )


def per_device(tokens, gain_in, expert_ids, gate_weights, w_gate, w_up, w_down, gain_out):
    own_rows, width = tokens.shape
    top = expert_ids.shape[1]
    experts = w_gate.shape[0] * lax.axis_size("ep")
    capacity = 2 * own_rows * top // experts
    halves = lax.axis_size("tp")
    x_float = tokens.astype(jnp.float32)
    normed = (
        x_float * lax.rsqrt(jnp.mean(x_float * x_float, axis=1, keepdims=True) + EPS) * gain_in
    ).astype(jnp.bfloat16)
    slots = block_slots(expert_ids, own_rows, experts)
    first = lax.axis_index("tp") * own_rows
    own_ids = lax.dynamic_slice_in_dim(expert_ids, first, own_rows, 0)
    own_slots = lax.dynamic_slice_in_dim(slots, first, own_rows, 0)
    position = (own_ids * capacity + own_slots).reshape(-1)
    source_rows = jnp.repeat(normed, top, axis=0)
    outgoing = jnp.zeros((experts * capacity, width), jnp.bfloat16).at[position].set(source_rows)
    outgoing = outgoing.reshape(experts, capacity, width)
    gate_all, up_all, down_all = side_by_side((w_gate, w_up, w_down), "tp", 2, 0)
    block = gate_all.shape[2] // halves
    arrived = lax.all_to_all(outgoing, "ep", split_axis=0, concat_axis=0, tiled=True)
    hidden = swiglu_rows(arrived, gate_all[0], up_all[0])
    summed = jnp.zeros(arrived.shape, jnp.float32)
    for index in range(halves):
        part = down_block(
            hidden[..., index * block : (index + 1) * block],
            down_all[0][:, index * block : (index + 1) * block],
        )
        summed = summed + lax.optimization_barrier(part.astype(jnp.bfloat16)).astype(jnp.float32)
    returned = lax.all_to_all(
        summed.astype(jnp.bfloat16), "ep", split_axis=0, concat_axis=0, tiled=True
    )
    table = returned.reshape(-1, width)
    own_gates = lax.dynamic_slice_in_dim(gate_weights, first, own_rows, 0)
    picked = table[own_ids * capacity + own_slots].astype(jnp.float32)
    combined = jnp.sum(own_gates[:, :, None] * picked, axis=1)
    inverse = lax.rsqrt(jnp.mean(combined * combined, axis=1, keepdims=True) + EPS)
    scaled = lax.all_to_all(
        (combined * inverse).astype(jnp.bfloat16), "tp", split_axis=1, concat_axis=0, tiled=True
    ).astype(jnp.float32)
    mixed = (scaled * gain_out).astype(jnp.bfloat16)
    return mixed


def solution(mesh):
    placed = (
        P(("grp", "ep", "tp"), None),
        P(),
        P(("grp", "ep"), None),
        P(("grp", "ep"), None),
        P("ep", None, "tp"),
        P("ep", None, "tp"),
        P("ep", None, "tp"),
        P("tp"),
    )
    return jax.shard_map(
        per_device, mesh=mesh, in_specs=placed, out_specs=P(("grp", "ep"), "tp"), check_vma=False
    )
```

profile of v0, /device:TPU:33, one launch (start us, length us, event | category | flops | bytes accessed | tf_op | source)
XLA Modules:
  0.0 495.0 jit_solution(18254187319409465269)
XLA Ops:
  6.6 0.9 copy.22
  7.5 0.2 eq.29
  7.9 2.4 reduce-window.6
  10.3 0.3 slice_reduce_fusion
  10.8 0.2 reshape.92
  11.2 0.3 fusion
  11.5 0.3 fusion.2
  11.8 1.3 broadcast_in_dim.7
  13.1 2.2 reshape.112
  15.4 7.3 %scatter_custom_fusion = bf16[1024,2048]{1,0:T(8,128)(2,1)} fusion(s32[512]{0:T(512)S(1)} %bitcast.53, bf16[512,2048]{1,0:T(8,128)(2,1)} %reshape.112, bf16[]{:T(256)} %constant.7.clone.1), kind=kCustom, calls=%fused_computation.23 | custom fusion | bytes 4194816 | tf_op jit(solution)/shard_map/scatter | solution.py:58
  22.7 29.9 %all-to-all-start = ((bf16[64,16,2048]{2,1,0:T(8,128)(2,1)}), bf16[64,16,2048]{2,1,0:T(8,128)(2,1)}, u32[]{:S(2)}, u32[]{:S(2)}) async-start(bf16[64,16,2048]{2,1,0:T(8,128)(2,1)} %bitcast.49), calls=%async_computation | async-start | bytes 8388608 | tf_op jit(solution)/shard_map/all_to_all | solution.py:62
  52.6 0.2 all-gather.2.cloned.1.call-start
  52.9 2.0 pad_maximum_fusion
  54.9 26.9 %all-gather.2.cloned.1.call-done = bf16[3,2048,512]{2,1,0:T(8,128)(2,1)} async-done(((bf16[3,2048,256]{2,1,0:T(8,128)(2,1)}), bf16[3,2048,512]{2,1,0:T(8,128)(2,1)}) %all-gather.2.cloned.1.call-update) | async-done | bytes 6291472 | tf_op jit(solution)/shard_map/all_gather | solution.py:12
  81.8 1.7 slice_bitcast_fusion
  83.5 152.0 %all-to-all-done = bf16[64,16,2048]{2,1,0:T(8,128)(2,1)} async-done(((bf16[64,16,2048]{2,1,0:T(8,128)(2,1)}), bf16[64,16,2048]{2,1,0:T(8,128)(2,1)}, u32[]{:S(2)}, u32[]{:S(2)}) %all-to-all-start) | async-done | bytes 4194336 | tf_op jit(solution)/shard_map/all_to_all | solution.py:62
  235.5 5.2 %fusion.4 = f32[1024,512]{1,0:T(8,128)S(1)} fusion(bf16[1024,2048]{1,0:T(8,128)(2,1)} %bitcast.3, bf16[3,2048,512]{2,1,0:T(8,128)(2,1)} %all-gather.2.cloned.1.call-done), kind=kOutput, calls=%fused_computation.16 | convolution fusion | flops 2147483648 | bytes 8388608 | tf_op jit(solution)/shard_map/dot_general | solution.py:27
  240.7 5.4 %multiply_convert_fusion.1 = bf16[1024,512]{1,0:T(8,128)(2,1)S(1)} fusion(f32[1024,512]{1,0:T(8,128)S(1)} %fusion.4, bf16[1024,2048]{1,0:T(8,128)(2,1)} %bitcast.3, bf16[3,2048,512]{2,1,0:T(8,128)(2,1)} %all-gather.2.cloned.1.call-done), kind=kOutput, calls=%fused_computation.22 | convolution fusion | flops 2150629376 | bytes 9437184 | tf_op jit(solution)/shard_map/dot_general | solution.py:28
  246.2 1.3 convolution_convert_fusion.1
  247.4 1.3 convolution_convert_fusion
  248.7 3.9 add_convert_fusion
  252.7 13.2 %all-to-all-start.1 = ((bf16[64,16,2048]{2,1,0:T(8,128)(2,1)}), bf16[64,16,2048]{2,1,0:T(8,128)(2,1)}, u32[]{:S(2)}, u32[]{:S(2)}) async-start(bf16[64,16,2048]{2,1,0:T(8,128)(2,1)} %add_convert_fusion), calls=%async_computation.1 | async-start | bytes 8388608 | tf_op jit(solution)/shard_map/all_to_all | solution.py:71
  266.2 182.6 %all-to-all-done.1 = bf16[64,16,2048]{2,1,0:T(8,128)(2,1)} async-done(((bf16[64,16,2048]{2,1,0:T(8,128)(2,1)}), bf16[64,16,2048]{2,1,0:T(8,128)(2,1)}, u32[]{:S(2)}, u32[]{:S(2)}) %all-to-all-start.1) | async-done | bytes 4194336 | tf_op jit(solution)/shard_map/all_to_all | solution.py:71
  448.9 7.1 %gather_fusion = bf16[512,2048]{1,0:T(8,128)(2,1)S(1)} fusion(bf16[1024,2048]{1,0:T(8,128)(2,1)} %bitcast.10, s32[1024]{0:T(1024)S(1)} %pad_clamp_fusion), kind=kCustom, calls=%fused_computation | custom fusion | bytes 4196352 | tf_op jit(solution)/shard_map/gather | solution.py:76
  456.0 4.0 reshape.118
  460.0 8.9 %multiply_reduce_fusion = f32[256,2048]{1,0:T(8,128)S(1)} fusion(f32[256,2,2048]{2,1,0:T(2,128)} %reshape.118, f32[256,2]{1,0:T(8,128)S(1)} %copy.21), kind=kLoop, calls=%fused_computation.3 | loop fusion | flops 1572864 | bytes 6293504 | tf_op jit(solution)/shard_map/reduce_sum | solution.py:77
  468.9 1.9 copy.26
  470.8 0.2 multiply_reduce_fusion.1
  471.0 1.4 copy-done.1
  472.5 10.7 %all_to_all.20 = bf16[256,2,1024]{0,2,1:T(8,128)(2,1)S(1)} all-to-all(bf16[256,2,1024]{0,2,1:T(8,128)(2,1)S(1)} %multiply_convert_fusion), channel_id=1, replica_groups=mesh['grp'=2,'ep'=64,'tp'=2] {'tp'}, dimensions={1} | all-to-all | bytes 2097152 | tf_op jit(solution)/shard_map/all_to_all | solution.py:79
  483.4 1.9 copy.27
  485.3 2.8 fusion.5
  (32 shorter events, 1.3 us)
Async XLA Ops:
  6.5 259.5 %copy-start = (f32[512,2]{0,1:T(2,128)S(1)}, f32[512,2]{0,1:T(2,128)}, u32[]{:S(2)}) copy-start(f32[512,2]{0,1:T(2,128)} %param.11) | copy-start | bytes 12292
  6.6 4.7 copy-start.2
  6.6 5.0 %copy-start.6 = (f32[2048]{0:T(1024)S(1)}, f32[2048]{0:T(1024)}, u32[]{:S(2)}) copy-start(f32[2048]{0:T(1024)} %param.9) | copy-start | bytes 24580
  22.7 30.1 %copy-start.3 = (bf16[1,2048,256]{2,1,0:T(8,128)(2,1)S(1)}, bf16[1,2048,256]{2,1,0:T(8,128)(2,1)}, u32[]{:S(2)}) copy-start(bf16[1,2048,256]{2,1,0:T(8,128)(2,1)} %param.14) | copy-start | bytes 3145732
  22.7 30.2 %copy-start.4 = (bf16[1,2048,256]{2,1,0:T(8,128)(2,1)S(1)}, bf16[1,2048,256]{2,1,0:T(8,128)(2,1)}, u32[]{:S(2)}) copy-start(bf16[1,2048,256]{2,1,0:T(8,128)(2,1)} %param.13) | copy-start | bytes 3145732
  22.7 30.2 %copy-start.5 = (bf16[1,2048,256]{2,1,0:T(8,128)(2,1)S(1)}, bf16[1,2048,256]{2,1,0:T(8,128)(2,1)}, u32[]{:S(2)}) copy-start(bf16[1,2048,256]{2,1,0:T(8,128)(2,1)} %param.12) | copy-start | bytes 3145732
  22.7 212.8 %all-to-all-start = ((bf16[64,16,2048]{2,1,0:T(8,128)(2,1)}), bf16[64,16,2048]{2,1,0:T(8,128)(2,1)}, u32[]{:S(2)}, u32[]{:S(2)}) async-start(bf16[64,16,2048]{2,1,0:T(8,128)(2,1)} %bitcast.49), calls=%async_computation | async-start | bytes 8388608 | tf_op jit(solution)/shard_map/all_to_all | solution.py:62
  52.6 29.2 %all-gather.2.cloned.1.call-start = ((), (), s32[]{:S(2)}) async-start(), calls=%async_computation.3 | async-start | bytes 9437184 | tf_op jit(solution)/shard_map/all_gather | solution.py:12
  252.7 196.2 %all-to-all-start.1 = ((bf16[64,16,2048]{2,1,0:T(8,128)(2,1)}), bf16[64,16,2048]{2,1,0:T(8,128)(2,1)}, u32[]{:S(2)}, u32[]{:S(2)}) async-start(bf16[64,16,2048]{2,1,0:T(8,128)(2,1)} %add_convert_fusion), calls=%async_computation.1 | async-start | bytes 8388608 | tf_op jit(solution)/shard_map/all_to_all | solution.py:71
  470.8 1.6 copy-start.1
  483.4 1.9 copy-start.7
Sparse Core Ops, SparseCore 0:
  55.2 26.5 all-gather.1
where the time goes:
time: 495 us
  waiting for transfers between devices  362 us (73%)
  starting transfers between devices  43.4 us (9%)
  local copies, waits for them, and re-layouts  31.1 us (6%)
  other arithmetic  21.4 us (4%)
  between operations  13.7 us (3%)
  matrix products  13.2 us (3%)
  blocking collectives  10.7 us (2%)
    all_to_all x1, waiting for transfers between devices, per_device(): lax.all_to_all(summed.astype(jnp.bfloat16), 'ep', split_axis=0, concat_ax...  183 us
    all_to_all x1, waiting for transfers between devices, per_device(): lax.all_to_all(outgoing, 'ep', split_axis=0, concat_axis=0, tiled=True)  152 us
    all_to_all x1, starting transfers between devices, per_device(): lax.all_to_all(outgoing, 'ep', split_axis=0, concat_axis=0, tiled=True)  29.9 us
    all_gather x1, waiting for transfers between devices, side_by_side(): filled = lax.all_gather(both, axis, axis=dim, tiled=True)  26.9 us
    all_to_all x1, starting transfers between devices, per_device(): lax.all_to_all(summed.astype(jnp.bfloat16), 'ep', split_axis=0, concat_ax...  13.2 us
    all_to_all x1, blocking collectives, per_device(): lax.all_to_all((combined * inverse).astype(jnp.bfloat16), 'tp', split_axi...  10.7 us
  transfers between devices with their start and end apart: 3, of which 3 were waited for; matrix products, arithmetic and copies ran while one was open for 1% of the time, Pallas kernels for 0%

commit v1 on v0

v1 whole, which is shorter than its diff:
```python
import functools

import jax
import jax.numpy as jnp
from jax import lax
from jax.experimental import pallas as pl
from jax.experimental.pallas import tpu as pltpu
from jax.sharding import PartitionSpec as P

EPS = 1e-06
COLUMNS = 4
MESH = pl.DeviceIdType.MESH
VMEM = pl.BlockSpec(memory_space=pltpu.VMEM)
ANY = pl.BlockSpec(memory_space=pl.ANY)
VMEM_LIMIT = 60 * 1024 * 1024


class Plan:
    def __init__(self, rows, width, members, capacity, columns):
        self.rows, self.width, self.members, self.cap, self.X = rows, width, members, capacity, columns
        self.Z = members // columns
        self.H = self.Z // 2
        self.slots = columns * capacity
        self.piece = self.slots // 2
        self.prefix = [0] + [
            min(rows, (self.H - d) * self.slots + self.slots // 2) for d in range(1, self.H + 1)
        ] + [0]
        self.pieces = [n // self.piece for n in self.prefix]
        self.offset = [sum(self.prefix[:d]) for d in range(self.H + 2)]
        self.total = sum(self.prefix)
        self.most = max(self.pieces)

    def me(self):
        ep = lax.axis_index("ep")
        return ep // self.X, ep % self.X

    def at(self, z, x):
        return lax.rem(z + 2 * self.Z, self.Z) * self.X + lax.rem(x + 2 * self.X, self.X)


def remote(src, dst, send, recv, **where):
    return pltpu.make_async_remote_copy(
        src_ref=src, dst_ref=dst, send_sem=send, recv_sem=recv, device_id=where, device_id_type=MESH
    )


def greet(plan, partner):
    z, x = plan.me()
    barrier = pltpu.get_barrier_semaphore()
    peers = [{"ep": plan.at(z + 1, x)}, {"ep": plan.at(z - 1, x)}]
    peers += [{"ep": plan.at(z, x + r)} for r in range(1, plan.X)]
    if partner:
        peers.append({"tp": 1 - lax.axis_index("tp")})
    for peer in peers:
        pl.semaphore_signal(barrier, inc=1, device_id=peer, device_id_type=MESH)
    pl.semaphore_wait(barrier, len(peers))


def iota(shape, dim):
    return lax.broadcasted_iota(jnp.int32, shape, dim)


def sort_kernel(plan, x_ref, gain_ref, ids_ref, gates_ref, plus_ref, minus_ref, meta_ref, normed):
    rows, X, Z, H = plan.rows, plan.X, plan.Z, plan.H
    z, _ = plan.me()
    step = 32

    def norm_step(i, carry):
        here = pl.ds(pl.multiple_of(i * step, step), step)
        x = x_ref[here, :].astype(jnp.float32)
        scale = lax.rsqrt(jnp.mean(x * x, axis=1, keepdims=True) + EPS)
        normed[here, :] = (x * scale * gain_ref[...]).astype(jnp.bfloat16)
        return carry

    lax.fori_loop(0, rows // step, norm_step, 0)

    own = pl.ds(pl.multiple_of(lax.axis_index("tp") * rows, rows), rows)
    ids, gates = ids_ref[own, :], gates_ref[own, :]
    square = (rows, rows)
    sub, lane = iota(square, 0), iota(square, 1)
    eye = sub == lane

    def as_row(column):
        return jnp.sum(jnp.where(eye, column, 0.0), axis=0, keepdims=True)

    def count(mask, axis):
        return jnp.sum(jnp.where(mask, 1.0, 0.0), axis=axis, keepdims=True)

    cols = [ids[:, k : k + 1].astype(jnp.float32) for k in range(2)]
    rws = [as_row(c) for c in cols]
    gcols = [gates[:, k : k + 1] for k in range(2)]
    grws = [as_row(g) for g in gcols]
    q_col, q_row, key_col, key_row = [], [], [[], []], [[], []]
    for k in range(2):
        slot_row = count((sub < lane) & (cols[0] == rws[k]), 0) + count((sub < lane) & (cols[1] == rws[k]), 0)
        slot_col = count((lane < sub) & (rws[0] == cols[k]), 1) + count((lane < sub) & (rws[1] == cols[k]), 1)
        q_row.append(rws[k] * plan.cap + slot_row)
        q_col.append(cols[k] * plan.cap + slot_col)
        for expert, keys in ((rws[k], key_row), (cols[k], key_col)):
            e = expert.astype(jnp.int32)
            ahead = e // X - z
            ahead = jnp.where(ahead < 0, ahead + Z, ahead)
            first = e % X < X // 2
            up = jnp.where((ahead < H) | ((ahead == H) & first), ahead, 0)
            down = jnp.where((ahead > H) | ((ahead == H) & ~first), Z - ahead, 0)
            keys[0].append(up.astype(jnp.float32))
            keys[1].append(down.astype(jnp.float32))
    for k in range(2):
        meta_ref[2, k : k + 1, :] = q_row[k]
        meta_ref[2, 2 + k : 3 + k, :] = grws[k]
    for way, out in ((0, plus_ref), (1, minus_ref)):
        far_col = jnp.maximum(*key_col[way])
        far_row = jnp.maximum(*key_row[way])
        rank_row = count((far_col > far_row) | ((far_col == far_row) & (sub < lane)), 0)
        rank_col = count((far_row > far_col) | ((far_row == far_col) & (lane < sub)), 1)
        meta_ref[2, 4 + way : 5 + way, :] = rank_row
        chosen = rank_col == lane.astype(jnp.float32)
        for k in range(2):
            meta_ref[way, k : k + 1, :] = jnp.sum(jnp.where(chosen, q_col[k], 0.0), axis=0, keepdims=True)
            meta_ref[way, 2 + k : 3 + k, :] = jnp.sum(jnp.where(chosen, gcols[k], 0.0), axis=0, keepdims=True)
        meta_ref[way, 4:8, :] = jnp.zeros((4, rows), jnp.float32)
        order = jnp.where(sub.astype(jnp.float32) == rank_row, 1.0, 0.0).astype(jnp.bfloat16)
        for c in range(0, plan.width, 512):
            n = min(512, plan.width)
            out[:, c : c + n] = jnp.dot(
                order, normed[:, c : c + n], preferred_element_type=jnp.float32
            ).astype(jnp.bfloat16)
    meta_ref[2, 6:8, :] = jnp.zeros((2, rows), jnp.float32)


def sort_tokens(plan, tokens, gain_in, expert_ids, gate_weights):
    rows, width = plan.rows, plan.width
    return pl.pallas_call(
        functools.partial(sort_kernel, plan),
        out_shape=(
            jax.ShapeDtypeStruct((rows, width), jnp.bfloat16),
            jax.ShapeDtypeStruct((rows, width), jnp.bfloat16),
            jax.ShapeDtypeStruct((3, 8, rows), jnp.float32),
        ),
        in_specs=[VMEM] * 4,
        out_specs=(VMEM,) * 3,
        scratch_shapes=[pltpu.VMEM((rows, width), jnp.bfloat16)],
        compiler_params=pltpu.CompilerParams(vmem_limit_bytes=VMEM_LIMIT),
        name="sort_tokens",
    )(tokens, gain_in.reshape(1, width), expert_ids, gate_weights)


def hits(plan, meta, n, z, way, d, weighted):
    slots, cap = plan.slots, plan.cap
    slot = iota((slots, n), 0)
    base = z * slots
    total = jnp.zeros((slots, n), jnp.float32)
    for k in range(2):
        match = meta[k : k + 1, :n].astype(jnp.int32) - base == slot
        if d == plan.H:
            match = match & (slot < slots // 2 if way == 0 else slot >= slots // 2)
        total = total + jnp.where(match, meta[2 + k : 3 + k, :n] if weighted else 1.0, 0.0)
    return total


def dispatch_kernel(
    plan,
    plus_ref, minus_ref, meta_ref, wg_ref, wu_ref, wd_ref,
    arrived_ref, og_ref, ou_ref, od_ref, metas_ref,
    ring, metas, stage, zsend, zrecv, msend, mrecv, xsend, xrecv, lsem, wsend, wrecv,
):
    X, Z, H, cap, piece = plan.X, plan.Z, plan.H, plan.cap, plan.piece
    z, x = plan.me()
    greet(plan, True)
    other = 1 - lax.axis_index("tp")

    own = (plus_ref, minus_ref)
    ahead = (plan.at(z + 1, x), plan.at(z - 1, x))

    def passing(way, d, p):
        dst = ring.at[way, pl.ds(plan.offset[d] + p * piece, piece), :]
        if d == 1:
            src = own[way].at[pl.ds(p * piece, piece), :]
        else:
            src = ring.at[way, pl.ds(plan.offset[d - 1] + p * piece, piece), :]
        return remote(src, dst, zsend.at[way, d - 1, p], zrecv.at[way, d - 1, p], ep=ahead[way])

    def passing_meta(way, d):
        src = meta_ref.at[way] if d == 1 else metas.at[way, d - 2]
        return remote(src, metas.at[way, d - 1], msend.at[way, d - 1], mrecv.at[way, d - 1], ep=ahead[way])

    def hand_over(k, r):
        column = lax.rem(x + r, X)
        src = stage.at[k, pl.ds(pl.multiple_of(column * cap, cap), cap), :]
        block = pl.multiple_of(plan.at(z + k, x) * cap, cap)
        dst = arrived_ref.at[pl.ds(block, cap), :]
        if r == 0:
            return pltpu.make_async_copy(src, dst, lsem.at[k])
        return remote(src, dst, xsend.at[k, r], xrecv.at[k, r], ep=plan.at(z, x + r))

    def pick(source, meta, n, way, d, k):
        chosen = hits(plan, meta, n, z, way, d, False).astype(jnp.bfloat16)
        wide = min(512, plan.width)

        def columns(c, carry):
            here = pl.ds(pl.multiple_of(c * wide, wide), wide)
            found = jnp.dot(chosen, source[:n, here], preferred_element_type=jnp.float32)
            found = found.astype(jnp.bfloat16)
            if d == H:
                half = plan.slots // 2
                lo = 0 if way == 0 else half
                stage[k, lo : lo + half, here] = found[lo : lo + half, :]
            else:
                stage[k, :, here] = found
            return carry

        lax.fori_loop(0, plan.width // wide, columns, 0)

    for way in range(2):
        passing_meta(way, 1).start()
    for p in range(plan.pieces[1]):
        for way in range(2):
            passing(way, 1, p).start()
    weights = [
        remote(src, dst, wsend.at[i], wrecv.at[i], tp=other)
        for i, (src, dst) in enumerate(((wg_ref, og_ref), (wu_ref, ou_ref), (wd_ref, od_ref)))
    ]
    for copy in weights:
        copy.start()

    def send_rows(k):
        for r in range(1, X):
            hand_over(k, r).start()
        hand_over(k, 0).start()

    pick(plus_ref, meta_ref[0], plan.rows, 0, 0, 0)
    ready = [0]
    for d in range(1, H + 1):
        for way in range(2):
            passing_meta(way, d).wait_recv()
            if d < H:
                passing_meta(way, d + 1).start()
        for p in range(plan.pieces[d]):
            for way in range(2):
                passing(way, d, p).wait_recv()
                if p < plan.pieces[d + 1]:
                    passing(way, d + 1, p).start()
        for k in ready:
            send_rows(k)
        ready = []
        for way in range(2):
            k = (Z - d if way == 0 else d) % Z
            n = plan.prefix[d]
            pick(ring.at[way, pl.ds(plan.offset[d], n), :], metas[way, d - 1], n, way, d, k)
            if d < H:
                ready.append(k)
    metas_ref[...] = metas[...]
    for k in [H] + ready:
        send_rows(k)

    for k in range(Z):
        for r in range(1, X):
            hand_over(k, r).wait_recv()
        hand_over(k, 0).wait()
    for copy in weights:
        copy.wait()
    for k in range(Z):
        for r in range(1, X):
            hand_over(k, r).wait_send()
    for d in range(1, H + 1):
        for way in range(2):
            passing_meta(way, d).wait_send()
            for p in range(plan.pieces[d]):
                passing(way, d, p).wait_send()


def dispatch(plan, plus, minus, meta, w_gate, w_up, w_down):
    X, Z, H, rows, width = plan.X, plan.Z, plan.H, plan.rows, plan.width
    dma = pltpu.SemaphoreType.DMA
    return pl.pallas_call(
        functools.partial(dispatch_kernel, plan),
        out_shape=(
            jax.ShapeDtypeStruct((plan.members * plan.cap, width), jnp.bfloat16),
            jax.ShapeDtypeStruct(w_gate.shape, w_gate.dtype),
            jax.ShapeDtypeStruct(w_up.shape, w_up.dtype),
            jax.ShapeDtypeStruct(w_down.shape, w_down.dtype),
            jax.ShapeDtypeStruct((2, H, 8, rows), jnp.float32),
        ),
        in_specs=[VMEM, VMEM, VMEM, ANY, ANY, ANY],
        out_specs=(ANY, ANY, ANY, ANY, VMEM),
        scratch_shapes=[
            pltpu.VMEM((2, plan.total, width), jnp.bfloat16),
            pltpu.VMEM((2, H, 8, rows), jnp.float32),
            pltpu.VMEM((Z, plan.slots, width), jnp.bfloat16),
            dma((2, H, plan.most)), dma((2, H, plan.most)), dma((2, H)), dma((2, H)),
            dma((Z, X)), dma((Z, X)), dma((Z,)), dma((3,)), dma((3,)),
        ],
        compiler_params=pltpu.CompilerParams(
            collective_id=0, has_side_effects=True, vmem_limit_bytes=VMEM_LIMIT
        ),
        name="dispatch",
    )(plus, minus, meta, w_gate, w_up, w_down)


def combine_kernel(
    plan,
    out_ref, meta_ref, metas_ref,
    scaled_ref,
    back, leaving, rows_in, spread, doubled, zsend, zrecv, xsend, xrecv, lsem,
):
    X, Z, H, cap, piece, width = plan.X, plan.Z, plan.H, plan.cap, plan.piece, plan.width
    z, x = plan.me()
    greet(plan, False)
    ahead = (plan.at(z - 1, x), plan.at(z + 1, x))
    wide = min(512, width)

    def give_back(k, r):
        block = pl.multiple_of(plan.at(z + k, x + r) * cap, cap)
        dst = rows_in.at[k, pl.ds(pl.multiple_of(x * cap, cap), cap), :]
        src = out_ref.at[pl.ds(block, cap), :]
        if r == 0:
            return pltpu.make_async_copy(src, dst, lsem.at[k])
        return remote(src, dst, xsend.at[k, r], xrecv.at[k, r], ep=plan.at(z, x + r))

    def passing(way, d, p):
        here = pl.ds(plan.offset[d] + p * piece, piece)
        return remote(
            leaving.at[way, here, :], back.at[way, here, :],
            zsend.at[way, d - 1, p], zrecv.at[way, d - 1, p], ep=ahead[way],
        )

    def sources(d):
        return sorted({(Z - d) % Z, d % Z})

    for d in range(H, -1, -1):
        for k in sources(d):
            for r in range(X):
                give_back(k, r).start()

    def prepare(way, d, k, meta, n):
        w = hits(plan, meta, n, z, way, d, True)
        high = w.astype(jnp.bfloat16).astype(jnp.float32)
        both = jnp.concatenate([high, w - high], axis=0)
        spread[way, :n, :] = both.T.astype(jnp.bfloat16)
        doubled[way, : plan.slots, :] = rows_in[k]
        doubled[way, plan.slots :, :] = rows_in[k]

    def wait_rows(k):
        for r in range(1, X):
            give_back(k, r).wait_recv()
        give_back(k, 0).wait()

    for d in range(H, 0, -1):
        for k in sources(d):
            wait_rows(k)
        for way in range(2):
            prepare(way, d, (Z - d if way == 0 else d) % Z, metas_ref[way, d - 1], plan.prefix[d])

        def one(p, carry, joined, d=d):
            for way in range(2):
                if joined:
                    passing(way, d + 1, p).wait_recv()
                place = spread[way, pl.ds(pl.multiple_of(p * piece, piece), piece), :]
                mine = pl.ds(pl.multiple_of(plan.offset[d] + p * piece, piece), piece)
                for c in range(0, width, wide):
                    part = jnp.dot(
                        place, doubled[way, :, c : c + wide], preferred_element_type=jnp.float32
                    )
                    if joined:
                        there = pl.ds(pl.multiple_of(plan.offset[d + 1] + p * piece, piece), piece)
                        part = part + back[way, there, c : c + wide].astype(jnp.float32)
                    leaving[way, mine, c : c + wide] = part.astype(jnp.bfloat16)
            for way in range(2):
                passing(way, d, p).start()
            return carry

        old, new = plan.pieces[d + 1], plan.pieces[d]
        if new > old:
            lax.fori_loop(old, new, functools.partial(one, joined=False), 0)
        if old:
            lax.fori_loop(0, old, functools.partial(one, joined=True), 0)

    wait_rows(0)
    prepare(0, 0, 0, meta_ref[2], plan.rows)
    for way in range(2):
        def arrive(p, carry, way=way):
            passing(way, 1, p).wait_recv()
            return carry

        lax.fori_loop(0, plan.pieces[1], arrive, 0)
    ranks = meta_ref[2]
    order = []
    for way in range(2):
        slot = iota((plan.rows, plan.rows), 0).astype(jnp.float32)
        order.append(jnp.where(slot == ranks[4 + way : 5 + way, :], 1.0, 0.0).T.astype(jnp.bfloat16))
    total = jnp.zeros((plan.rows, 1), jnp.float32)
    first = plan.offset[1]
    sums = []
    for c in range(0, width, wide):
        part = jnp.dot(spread[0], doubled[0, :, c : c + wide], preferred_element_type=jnp.float32)
        for way in range(2):
            part = part + jnp.dot(
                order[way], back[way, first : first + plan.rows, c : c + wide],
                preferred_element_type=jnp.float32,
            )
        sums.append(part)
        total = total + jnp.sum(part * part, axis=1, keepdims=True)
    inverse = lax.rsqrt(total / width + EPS)
    for i, c in enumerate(range(0, width, wide)):
        scaled_ref[:, c : c + wide] = (sums[i] * inverse).astype(jnp.bfloat16)

    for k in range(Z):
        for r in range(1, X):
            give_back(k, r).wait_send()
    for d in range(1, H + 1):
        for way in range(2):
            def gone(p, carry, way=way, d=d):
                passing(way, d, p).wait_send()
                return carry

            lax.fori_loop(0, plan.pieces[d], gone, 0)


def combine(plan, out, meta, metas):
    X, Z, H, rows, width = plan.X, plan.Z, plan.H, plan.rows, plan.width
    dma = pltpu.SemaphoreType.DMA
    return pl.pallas_call(
        functools.partial(combine_kernel, plan),
        out_shape=jax.ShapeDtypeStruct((rows, width), jnp.bfloat16),
        in_specs=[ANY, VMEM, VMEM],
        out_specs=VMEM,
        scratch_shapes=[
            pltpu.VMEM((2, plan.total, width), jnp.bfloat16),
            pltpu.VMEM((2, plan.total, width), jnp.bfloat16),
            pltpu.VMEM((Z, plan.slots, width), jnp.bfloat16),
            pltpu.VMEM((2, rows, 2 * plan.slots), jnp.bfloat16),
            pltpu.VMEM((2, 2 * plan.slots, width), jnp.bfloat16),
            dma((2, H, plan.most)), dma((2, H, plan.most)),
            dma((Z, X)), dma((Z, X)), dma((Z,)),
        ],
        compiler_params=pltpu.CompilerParams(
            collective_id=1, has_side_effects=True, vmem_limit_bytes=VMEM_LIMIT
        ),
        name="combine",
    )(out, meta, metas)


def expert_half(rows, gate_matrix, up_matrix, down_matrix):
    gated = jnp.dot(rows, gate_matrix, preferred_element_type=jnp.float32)
    upward = jnp.dot(rows, up_matrix, preferred_element_type=jnp.float32)
    hidden = (jax.nn.silu(gated) * upward).astype(jnp.bfloat16)
    part = lax.dot_general(
        hidden, down_matrix, (((1,), (1,)), ((), ())), preferred_element_type=jnp.float32
    )
    return lax.optimization_barrier(part.astype(jnp.bfloat16)).astype(jnp.float32)


def per_device(columns, tokens, gain_in, expert_ids, gate_weights, w_gate, w_up, w_down, gain_out):
    own_rows, width = tokens.shape
    members = lax.axis_size("ep")
    capacity = 2 * own_rows * expert_ids.shape[1] // members
    plan = Plan(own_rows, width, members, capacity, columns)
    plus, minus, meta = sort_tokens(plan, tokens, gain_in, expert_ids, gate_weights)
    arrived, o_gate, o_up, o_down, metas = dispatch(
        plan, plus, minus, meta, w_gate[0], w_up[0], w_down[0]
    )
    summed = expert_half(arrived, w_gate[0], w_up[0], w_down[0])
    summed = summed + expert_half(arrived, o_gate, o_up, o_down)
    scaled = combine(plan, summed.astype(jnp.bfloat16), meta, metas)
    scaled = lax.all_to_all(scaled, "tp", split_axis=1, concat_axis=0, tiled=True)
    return (scaled.astype(jnp.float32) * gain_out).astype(jnp.bfloat16)


def solution(mesh, columns=COLUMNS):
    placed = (
        P(("grp", "ep", "tp"), None),
        P(),
        P(("grp", "ep"), None),
        P(("grp", "ep"), None),
        P("ep", None, "tp"),
        P("ep", None, "tp"),
        P("ep", None, "tp"),
        P("tp"),
    )
    return jax.shard_map(
        functools.partial(per_device, columns),
        mesh=mesh, in_specs=placed, out_specs=P(("grp", "ep"), "tp"), check_vma=False,
    )
```

time: 495 us -> 380 us (0.77)
  waiting for transfers between devices: 362 us -> 0 us
  Pallas kernels: 0 us -> 330 us
  starting transfers between devices: 43.4 us -> 0 us
  local copies, waits for them, and re-layouts: 31.1 us -> 4.5 us
  between operations: 13.7 us -> 0.06 us
  other arithmetic: 21.4 us -> 8.95 us
  matrix products: 13.2 us -> 24.9 us
    all_to_all x2 -> x0, waiting for transfers between devices: 335 us -> none  [the longest x1 183 us: per_device(): lax.all_to_all(summed.astype(jnp.bfloat16), 'ep', split_axis=0, concat_ax...]
    pallas_call x0 -> x3, Pallas kernels: none -> 330 us  [the longest x1 179 us: dispatch(): pl.pallas_call(functools.partial(dispatch_kernel, plan), out_shape=(jax.S...]
    all_to_all x2 -> x0, starting transfers between devices: 43.1 us -> none  [the longest x1 29.9 us: per_device(): lax.all_to_all(outgoing, 'ep', split_axis=0, concat_axis=0, tiled=True)]
    all_gather x1 -> x0, waiting for transfers between devices: 26.9 us -> none  [side_by_side(): filled = lax.all_gather(both, axis, axis=dim, tiled=True)]
    dot_general x4, matrix products: 13.2 us -> 24.9 us  [the longest x2 18 us: expert_half(): lax.dot_general(hidden, down_matrix, (((1,), (1,)), ((), ())), preferred_...]
    reduce_sum x4 -> x0, other arithmetic: 9.55 us -> none  [the longest x1 8.88 us: per_device(): combined = jnp.sum(own_gates[:, :, None] * picked, axis=1)]
    scatter x1 -> x0, local copies, waits for them, and re-layouts: 7.32 us -> none  [per_device(): jnp.zeros((experts * capacity, width), jnp.bfloat16).at[position]]
    gather x1 -> x0, local copies, waits for them, and re-layouts: 7.13 us -> none  [per_device(): picked = table[own_ids * capacity + own_slots].astype(jnp.float32)]
  transfers between devices with their start and end apart: 3 -> 0, of which waited for: 3 -> 0; matrix products, arithmetic and copies ran while one was open for 1% -> 0% of each run, Pallas kernels for 0% -> 0%
where the time goes in v1:
time: 380 us
  Pallas kernels  330 us (87%)
  matrix products  24.9 us (7%)
  blocking collectives  11.6 us (3%)
  other arithmetic  8.95 us (2%)
  local copies, waits for them, and re-layouts  4.5 us (1%)
    pallas_call x1, Pallas kernels, dispatch(): pl.pallas_call(functools.partial(dispatch_kernel, plan), out_shape=(jax.S...  179 us
    pallas_call x1, Pallas kernels, combine(): pl.pallas_call(functools.partial(combine_kernel, plan), out_shape=jax.Sha...  146 us
    dot_general x2, matrix products, expert_half(): lax.dot_general(hidden, down_matrix, (((1,), (1,)), ((), ())), preferred_...  18 us
    all_to_all x1, blocking collectives, per_device(): lax.all_to_all(scaled, 'tp', split_axis=1, concat_axis=0, tiled=True)  11.6 us
    convert_element_type x1, other arithmetic, per_device(): scaled = combine(plan, summed.astype(jnp.bfloat16), meta, metas)  7.74 us

profile of v1, /device:TPU:33, one launch (start us, length us, event | category | flops | bytes accessed | tf_op | source)
XLA Modules:
  0.0 380.1 jit_solution(15910627977063824592)
XLA Ops:
  0.0 0.0 copy-start
  0.0 1.6 copy.12.ids_ref
  1.6 1.6 copy.13.gates_ref
  3.2 4.7 %sort_tokens.1 = (bf16[256,2048]{1,0:T(8,128)(2,1)}, bf16[256,2048]{1,0:T(8,128)(2,1)}, f32[3,8,256]{2,1,0:T(8,128)}) custom-call(bf16[256,2048]{1,0:T(8,128)(2,1)} %x_ref.1, f32[1,2048]{1,0:T(1,128)} %bitcast.33, s32[512,2]{1,0:T(8,128)} %copy.12.ids_ref, f32[512,2]{1,0:T(8,128)} %copy.13.gates_ref), custom_call_target="tpu_custom_call" | custom-call | tf_op jit(solution)/shard_map/sort_tokens/pallas_call | solution.py:133
  7.9 179.4 %dispatch.1 = (bf16[1024,2048]{1,0:T(8,128)(2,1)}, bf16[2048,256]{1,0:T(8,128)(2,1)}, bf16[2048,256]{1,0:T(8,128)(2,1)}, bf16[2048,256]{1,0:T(8,128)(2,1)}, f32[2,8,8,256]{3,2,1,0:T(8,128)}) custom-call(bf16[256,2048]{1,0:T(8,128)(2,1)} %get-tuple-element.13.plus_ref, bf16[256,2048]{1,0:T(8,128)(2,1)} %get-tuple-element.14.minus_ref, ...), custom_call_target="tpu_custom_call" | custom-call | tf_op jit(solution)/shard_map/dispatch/pallas_call | solution.py:275
  187.3 0.0 copy-start.4
  187.3 0.0 copy-start.6
  187.3 0.0 copy-done
  187.4 4.6 %fusion.18 = f32[1024,256]{1,0:T(8,128)} fusion(bf16[1024,2048]{1,0:T(8,128)(2,1)} %get-tuple-element.16, bf16[1,2048,256]{2,1,0:T(8,128)(2,1)S(1)} %copy-done), kind=kOutput, calls=%fused_computation.24 | convolution fusion | flops 1073741824 | bytes 6291456 | tf_op jit(solution)/shard_map/dot_general | solution.py:444
  192.0 0.0 copy-start.5
  192.0 0.0 copy-done.4
  192.0 0.0 copy-done.6
  192.0 2.2 fusion.22
  194.2 0.0 copy-done.5
  194.2 0.0 copy-start.1
  194.2 0.0 copy-start.2
  194.2 9.3 %convolution_convert_fusion = bf16[1024,2048]{1,0:T(8,128)(2,1)} fusion(bf16[2048,256]{1,0:T(8,128)(2,1)} %get-tuple-element.19, bf16[1024,2048]{1,0:T(8,128)(2,1)} %get-tuple-element.16, bf16[2048,256]{1,0:T(8,128)(2,1)S(1)} %copy-done.5, f32[1024,256]{1,0:T(8,128)} %fusion.22), kind=kOutput, calls=%fused_computation.1 | convolution fusion | flops 2151153664 | bytes 11534336 | tf_op jit(solution)/shard_map/dot_general | solution.py:447
  203.5 0.0 copy-done.1
  203.5 0.0 copy-done.2
  203.5 8.8 %convolution_convert_fusion.1 = bf16[1024,2048]{1,0:T(8,128)(2,1)} fusion(bf16[1024,2048]{1,0:T(8,128)(2,1)} %get-tuple-element.16, f32[1024,256]{1,0:T(8,128)} %fusion.18, bf16[1,2048,256]{2,1,0:T(8,128)(2,1)S(1)} %copy-done.2, bf16[1,2048,256]{2,1,0:T(8,128)(2,1)S(1)} %copy-done.1), kind=kOutput, calls=%fused_computation.2 | convolution fusion | flops 2151153664 | bytes 11534336 | tf_op jit(solution)/shard_map/dot_general | solution.py:447
  212.3 7.7 %add_convert_fusion.out_ref = bf16[1024,2048]{1,0:T(8,128)(2,1)} fusion(bf16[1024,2048]{1,0:T(8,128)(2,1)} %convolution_convert_fusion, bf16[1024,2048]{1,0:T(8,128)(2,1)} %convolution_convert_fusion.1), kind=kLoop, calls=%fused_computation | loop fusion | flops 8388608 | bytes 12582912 | tf_op jit(solution)/shard_map/convert_element_type | solution.py:464
  220.0 0.0 copy-start.3
  220.0 145.9 %combine.1 = bf16[256,2048]{1,0:T(8,128)(2,1)} custom-call(bf16[1024,2048]{1,0:T(8,128)(2,1)} %add_convert_fusion.out_ref, f32[3,8,256]{2,1,0:T(8,128)} %get-tuple-element.15.meta_ref, f32[2,8,8,256]{3,2,1,0:T(8,128)} %get-tuple-element.20.metas_ref), custom_call_target="tpu_custom_call" | custom-call | tf_op jit(solution)/shard_map/combine/pallas_call | solution.py:422
  365.9 1.3 copy.17
  367.2 11.6 %all_to_all.13 = bf16[256,2,1024]{2,0,1:T(8,128)(2,1)S(1)} all-to-all(bf16[256,2,1024]{2,0,1:T(8,128)(2,1)S(1)} %bitcast.28), channel_id=1, replica_groups=mesh['grp'=2,'ep'=64,'tp'=2] {'tp'}, dimensions={1} | all-to-all | bytes 2097152 | tf_op jit(solution)/shard_map/all_to_all | solution.py:465
  378.8 0.0 copy-done.3
  378.8 1.2 fusion
Async XLA Ops:
  0.0 187.4 %copy-start = (bf16[1,2048,256]{2,1,0:T(8,128)(2,1)S(1)}, bf16[1,2048,256]{2,1,0:T(8,128)(2,1)}, u32[]{:S(2)}) copy-start(bf16[1,2048,256]{2,1,0:T(8,128)(2,1)} %param.12) | copy-start | bytes 3145732
  187.3 4.7 %copy-start.4 = (bf16[1024,2048]{1,0:T(8,128)(2,1)S(1)}, bf16[1024,2048]{1,0:T(8,128)(2,1)}, u32[]{:S(2)}) copy-start(bf16[1024,2048]{1,0:T(8,128)(2,1)} %get-tuple-element.16) | copy-start | bytes 12582916
  187.3 4.7 %copy-start.6 = (bf16[2048,256]{1,0:T(8,128)(2,1)S(1)}, bf16[2048,256]{1,0:T(8,128)(2,1)}, u32[]{:S(2)}) copy-start(bf16[2048,256]{1,0:T(8,128)(2,1)} %get-tuple-element.17) | copy-start | bytes 3145732
  192.0 2.2 copy-start.5
  194.2 9.3 %copy-start.1 = (bf16[1,2048,256]{2,1,0:T(8,128)(2,1)S(1)}, bf16[1,2048,256]{2,1,0:T(8,128)(2,1)}, u32[]{:S(2)}) copy-start(bf16[1,2048,256]{2,1,0:T(8,128)(2,1)} %param.13) | copy-start | bytes 3145732
  194.2 9.3 %copy-start.2 = (bf16[1,2048,256]{2,1,0:T(8,128)(2,1)S(1)}, bf16[1,2048,256]{2,1,0:T(8,128)(2,1)}, u32[]{:S(2)}) copy-start(bf16[1,2048,256]{2,1,0:T(8,128)(2,1)} %param.14) | copy-start | bytes 3145732
  220.0 158.8 %copy-start.3 = (f32[1024]{0:T(1024)S(1)}, f32[1024]{0:T(1024)}, u32[]{:S(2)}) copy-start(f32[1024]{0:T(1024)} %param.15) | copy-start | bytes 12292

commit v2 on v1

v2 whole, which is shorter than its diff:
```python
import functools

import jax
import jax.numpy as jnp
from jax import lax
from jax.experimental import pallas as pl
from jax.experimental.pallas import tpu as pltpu
from jax.sharding import PartitionSpec as P

EPS = 1e-06
COLUMNS = 4
MESH = pl.DeviceIdType.MESH
VMEM = pl.BlockSpec(memory_space=pltpu.VMEM)
ANY = pl.BlockSpec(memory_space=pl.ANY)
VMEM_LIMIT = 60 * 1024 * 1024


class Plan:
    def __init__(self, rows, width, members, capacity, columns):
        self.rows, self.width, self.members, self.cap, self.X = rows, width, members, capacity, columns
        self.Z = members // columns
        self.H = self.Z // 2
        self.slots = columns * capacity
        self.piece = self.slots // 2
        self.prefix = [0] + [
            min(rows, (self.H - d) * self.slots + self.slots // 2) for d in range(1, self.H + 1)
        ] + [0]
        self.pieces = [n // self.piece for n in self.prefix]
        self.offset = [sum(self.prefix[:d]) for d in range(self.H + 2)]
        self.total = sum(self.prefix)
        self.most = max(self.pieces)

    def me(self):
        ep = lax.axis_index("ep")
        return ep // self.X, ep % self.X

    def at(self, z, x):
        return lax.rem(z + 2 * self.Z, self.Z) * self.X + lax.rem(x + 2 * self.X, self.X)


def remote(src, dst, send, recv, **where):
    return pltpu.make_async_remote_copy(
        src_ref=src, dst_ref=dst, send_sem=send, recv_sem=recv, device_id=where, device_id_type=MESH
    )


def greet(plan, partner):
    z, x = plan.me()
    barrier = pltpu.get_barrier_semaphore()
    peers = [{"ep": plan.at(z + 1, x)}, {"ep": plan.at(z - 1, x)}]
    peers += [{"ep": plan.at(z, x + r)} for r in range(1, plan.X)]
    if partner:
        peers.append({"tp": 1 - lax.axis_index("tp")})
    for peer in peers:
        pl.semaphore_signal(barrier, inc=1, device_id=peer, device_id_type=MESH)
    pl.semaphore_wait(barrier, len(peers))


def iota(shape, dim):
    return lax.broadcasted_iota(jnp.int32, shape, dim)


def sort_kernel(plan, x_ref, gain_ref, ids_ref, gates_ref, plus_ref, minus_ref, meta_ref, normed):
    rows, X, Z, H = plan.rows, plan.X, plan.Z, plan.H
    z, _ = plan.me()
    step = 32

    def norm_step(i, carry):
        here = pl.ds(pl.multiple_of(i * step, step), step)
        x = x_ref[here, :].astype(jnp.float32)
        scale = lax.rsqrt(jnp.mean(x * x, axis=1, keepdims=True) + EPS)
        normed[here, :] = (x * scale * gain_ref[...]).astype(jnp.bfloat16)
        return carry

    lax.fori_loop(0, rows // step, norm_step, 0)

    own = pl.ds(pl.multiple_of(lax.axis_index("tp") * rows, rows), rows)
    square = (rows, rows)
    sub, lane = iota(square, 0), iota(square, 1)
    eye = sub == lane

    def as_column(row):
        return jnp.sum(jnp.where(eye, row, 0.0), axis=1, keepdims=True)

    def count(mask, axis):
        return jnp.sum(jnp.where(mask, 1.0, 0.0), axis=axis, keepdims=True)

    rws = [ids_ref[k : k + 1, own].astype(jnp.float32) for k in range(2)]
    cols = [as_column(r) for r in rws]
    grws = [gates_ref[k : k + 1, own] for k in range(2)]
    gcols = [as_column(g) for g in grws]
    q_col, q_row, key_col, key_row = [], [], [[], []], [[], []]
    for k in range(2):
        slot_row = count((sub < lane) & (cols[0] == rws[k]), 0) + count((sub < lane) & (cols[1] == rws[k]), 0)
        slot_col = count((lane < sub) & (rws[0] == cols[k]), 1) + count((lane < sub) & (rws[1] == cols[k]), 1)
        q_row.append(rws[k] * plan.cap + slot_row)
        q_col.append(cols[k] * plan.cap + slot_col)
        for expert, keys in ((rws[k], key_row), (cols[k], key_col)):
            e = expert.astype(jnp.int32)
            ahead = e // X - z
            ahead = jnp.where(ahead < 0, ahead + Z, ahead)
            first = e % X < X // 2
            up = jnp.where((ahead < H) | ((ahead == H) & first), ahead, 0)
            down = jnp.where((ahead > H) | ((ahead == H) & ~first), Z - ahead, 0)
            keys[0].append(up.astype(jnp.float32))
            keys[1].append(down.astype(jnp.float32))
    for k in range(2):
        meta_ref[2, k : k + 1, :] = q_row[k]
        meta_ref[2, 2 + k : 3 + k, :] = grws[k]
    for way, out in ((0, plus_ref), (1, minus_ref)):
        far_col = jnp.maximum(*key_col[way])
        far_row = jnp.maximum(*key_row[way])
        rank_row = count((far_col > far_row) | ((far_col == far_row) & (sub < lane)), 0)
        rank_col = count((far_row > far_col) | ((far_row == far_col) & (lane < sub)), 1)
        meta_ref[2, 4 + way : 5 + way, :] = rank_row
        chosen = rank_col == lane.astype(jnp.float32)
        for k in range(2):
            meta_ref[way, k : k + 1, :] = jnp.sum(jnp.where(chosen, q_col[k], 0.0), axis=0, keepdims=True)
            meta_ref[way, 2 + k : 3 + k, :] = jnp.sum(jnp.where(chosen, gcols[k], 0.0), axis=0, keepdims=True)
        meta_ref[way, 4:8, :] = jnp.zeros((4, rows), jnp.float32)
        order = jnp.where(sub.astype(jnp.float32) == rank_row, 1.0, 0.0).astype(jnp.bfloat16)
        for c in range(0, plan.width, 512):
            n = min(512, plan.width)
            out[:, c : c + n] = jnp.dot(
                order, normed[:, c : c + n], preferred_element_type=jnp.float32
            ).astype(jnp.bfloat16)
    meta_ref[2, 6:8, :] = jnp.zeros((2, rows), jnp.float32)


def sort_tokens(plan, tokens, gain_in, expert_ids, gate_weights):
    rows, width = plan.rows, plan.width
    return pl.pallas_call(
        functools.partial(sort_kernel, plan),
        out_shape=(
            jax.ShapeDtypeStruct((rows, width), jnp.bfloat16),
            jax.ShapeDtypeStruct((rows, width), jnp.bfloat16),
            jax.ShapeDtypeStruct((3, 8, rows), jnp.float32),
        ),
        in_specs=[VMEM] * 4,
        out_specs=(VMEM,) * 3,
        scratch_shapes=[pltpu.VMEM((rows, width), jnp.bfloat16)],
        compiler_params=pltpu.CompilerParams(vmem_limit_bytes=VMEM_LIMIT),
        name="sort_tokens",
    )(tokens, gain_in.reshape(1, width), expert_ids.T, gate_weights.T)


def hits(plan, meta, n, z, way, d, weighted):
    slots, cap = plan.slots, plan.cap
    slot = iota((slots, n), 0)
    base = z * slots
    total = jnp.zeros((slots, n), jnp.float32)
    for k in range(2):
        match = meta[k : k + 1, :n].astype(jnp.int32) - base == slot
        if d == plan.H:
            match = match & (slot < slots // 2 if way == 0 else slot >= slots // 2)
        total = total + jnp.where(match, meta[2 + k : 3 + k, :n] if weighted else 1.0, 0.0)
    return total


def last_hop(plan, p):
    return max(d for d in range(1, plan.H + 1) if plan.pieces[d] > p)


def experts_kernel(
    plan,
    plus_ref, minus_ref, meta_ref, wg_ref, wu_ref, wd_ref,
    out_ref,
    ring, back, metas, stage, arrived, rows_in, spread, doubled, wg, wu, wd, halves, final,
    zsend, zrecv, bsend, brecv, msend, mrecv, xsend, xrecv, ysend, yrecv,
    wsend, wrecv, wown, fsem,
):
    X, Z, H, cap, piece = plan.X, plan.Z, plan.H, plan.cap, plan.piece
    rows, width, slots = plan.rows, plan.width, plan.slots
    wide = min(512, width)
    z, x = plan.me()
    core = lax.axis_index("tp")
    other = 1 - core
    greet(plan, True)

    own = (plus_ref, minus_ref)
    outward = (plan.at(z + 1, x), plan.at(z - 1, x))
    homeward = (outward[1], outward[0])
    held = range(H // 2, H - 1)

    def late(d, p):
        return d in held and last_hop(plan, p) == d

    def places(d):
        if d == 0:
            return [(0, 0)]
        if d == H:
            return [(0, Z - 1), (1, Z - 1)]
        return [(0, 2 * d - 1), (1, 2 * d)]

    def spots(d):
        return sorted({j for _, j in places(d)})

    def passing(way, d, p):
        dst = ring.at[way, pl.ds(plan.offset[d] + p * piece, piece), :]
        if d == 1:
            src = own[way].at[pl.ds(p * piece, piece), :]
        else:
            src = ring.at[way, pl.ds(plan.offset[d - 1] + p * piece, piece), :]
        return remote(src, dst, zsend.at[way, d - 1, p], zrecv.at[way, d - 1, p], ep=outward[way])

    def passing_meta(way, d):
        src = meta_ref.at[way] if d == 1 else metas.at[way, d - 2]
        return remote(src, metas.at[way, d - 1], msend.at[way, d - 1], mrecv.at[way, d - 1], ep=outward[way])

    def closer(way, d, p):
        here = pl.ds(plan.offset[d] + p * piece, piece)
        return remote(
            ring.at[way, here, :], back.at[way, here, :],
            bsend.at[way, d - 1, p], brecv.at[way, d - 1, p], ep=homeward[way],
        )

    def column(r):
        return pl.ds(pl.multiple_of(lax.rem(x + r, X) * cap, cap), cap)

    def hand_over(j, r):
        src, dst = stage.at[j, column(r), :], arrived.at[j, column(0), :]
        return remote(src, dst, xsend.at[j, r], xrecv.at[j, r], ep=plan.at(z, x + r))

    def give_back(j, r):
        src, dst = arrived.at[j, column(r), :], rows_in.at[j, column(0), :]
        return remote(src, dst, ysend.at[j, r], yrecv.at[j, r], ep=plan.at(z, x + r))

    picked, computed = [], []

    def flush(waiting, copy):
        for j in waiting:
            for r in range(1, X):
                copy(j, r).start()
            if copy is hand_over:
                arrived[j, column(0), :] = stage[j, column(0), :]
            else:
                rows_in[j, column(0), :] = arrived[j, column(0), :]
        waiting.clear()

    def pick(way, d, j):
        n = rows if d == 0 else plan.prefix[d]
        meta = meta_ref[0] if d == 0 else metas[way, d - 1]
        source = plus_ref if d == 0 else ring.at[way, pl.ds(plan.offset[d], n), :]
        chosen = hits(plan, meta, n, z, way, d, False).astype(jnp.bfloat16)

        def columns(c, carry):
            here = pl.ds(pl.multiple_of(c * wide, wide), wide)
            found = jnp.dot(chosen, source[:, here], preferred_element_type=jnp.float32)
            found = found.astype(jnp.bfloat16)
            if d == H:
                lo = way * (slots // 2)
                stage[j, lo : lo + slots // 2, here] = found[lo : lo + slots // 2, :]
            else:
                stage[j, :, here] = found
            return carry

        lax.fori_loop(0, width // wide, columns, 0)

    def pick_all(d):
        for way, j in places(d):
            pick(way, d, j)
        picked.extend(spots(d))

    def land(d):
        for p in range(plan.pieces[d]):
            if late(d, p):
                for way in range(2):
                    passing(way, d, p).wait_recv()
        pick_all(d)

    def expert(j, carry):
        hidden = []
        for half in range(2):
            gated = jnp.dot(arrived[j], wg[half], preferred_element_type=jnp.float32)
            upward = jnp.dot(arrived[j], wu[half], preferred_element_type=jnp.float32)
            hidden.append((gated / (1.0 + jnp.exp(-gated)) * upward).astype(jnp.bfloat16))
        step = min(256, width)

        def down(c, carry):
            here = pl.ds(pl.multiple_of(c * step, step), step)
            total = jnp.zeros((slots, step), jnp.float32)
            for half in range(2):
                part = lax.dot_general(
                    hidden[half], wd[half, here, :], (((1,), (1,)), ((), ())),
                    preferred_element_type=jnp.float32,
                )
                total = total + part.astype(jnp.bfloat16).astype(jnp.float32)
            arrived[j, :, here] = total.astype(jnp.bfloat16)
            return carry

        lax.fori_loop(0, width // step, down, 0)
        return carry

    def compute(d):
        for j in spots(d):
            for r in range(1, X):
                hand_over(j, r).wait_recv()
        lax.fori_loop(spots(d)[0], spots(d)[-1] + 1, expert, 0)
        computed.extend(spots(d))

    def prepare(way, d, j):
        n = rows if d == 0 else plan.prefix[d]
        meta = meta_ref[2] if d == 0 else metas[way, d - 1]
        w = hits(plan, meta, n, z, way, d, True)
        high = w.astype(jnp.bfloat16).astype(jnp.float32)
        spread[way, :n, :] = jnp.concatenate([high, w - high], axis=0).T.astype(jnp.bfloat16)
        doubled[way, :slots, :] = rows_in[j]
        doubled[way, slots:, :] = rows_in[j]

    def wait_rows(d):
        for j in spots(d):
            for r in range(1, X):
                give_back(j, r).wait_recv()

    def combine(d):
        wait_rows(d)
        for way, j in places(d):
            prepare(way, d, j)
        if d < H:
            for way in range(2):
                for p in range(plan.pieces[d + 1]):
                    passing(way, d + 1, p).wait_send()

        def one(p, carry, joined):
            for way in range(2):
                if joined:
                    closer(way, d + 1, p).wait_recv()
                place = spread[way, pl.ds(pl.multiple_of(p * piece, piece), piece), :]
                mine = pl.ds(pl.multiple_of(plan.offset[d] + p * piece, piece), piece)
                for c in range(0, width, wide):
                    part = jnp.dot(
                        place, doubled[way, :, c : c + wide], preferred_element_type=jnp.float32
                    )
                    if joined:
                        there = pl.ds(pl.multiple_of(plan.offset[d + 1] + p * piece, piece), piece)
                        part = part + back[way, there, c : c + wide].astype(jnp.float32)
                    ring[way, mine, c : c + wide] = part.astype(jnp.bfloat16)
            for way in range(2):
                closer(way, d, p).start()
            return carry

        old, new = plan.pieces[d + 1], plan.pieces[d]
        if new > old:
            lax.fori_loop(old, new, functools.partial(one, joined=False), 0)
        if old:
            lax.fori_loop(0, old, functools.partial(one, joined=True), 0)

    for way in range(2):
        passing_meta(way, 1).start()
    for p in range(plan.pieces[1]):
        for way in range(2):
            passing(way, 1, p).start()
    weights = []
    for i, (src, dst) in enumerate(((wg_ref, wg), (wu_ref, wu), (wd_ref, wd))):
        weights.append(remote(src, dst.at[1], wsend.at[i], wrecv.at[i], tp=other))
        weights.append(pltpu.make_async_copy(src, dst.at[0], wown.at[i]))
    for copy in weights:
        copy.start()
    pick_all(0)
    done = []
    for d in range(1, H):
        for way in range(2):
            passing_meta(way, d).wait_recv()
            passing_meta(way, d + 1).start()
        for p in range(plan.pieces[d]):
            if not late(d, p):
                for way in range(2):
                    passing(way, d, p).wait_recv()
                    if p < plan.pieces[d + 1] and not late(d + 1, p):
                        passing(way, d + 1, p).start()
        flush(picked, hand_over)
        flush(computed, give_back)
        if d == H - 1:
            for e in reversed(held):
                for p in range(plan.pieces[e]):
                    if late(e, p):
                        for way in range(2):
                            passing(way, e, p).start()
        if d not in held:
            pick_all(d)
        if d == 1:
            for copy in weights:
                copy.wait()
        if 0 <= d - 2 < H // 2:
            compute(d - 2)
            done.append(d - 2)
    flush(picked, hand_over)
    flush(computed, give_back)

    rest = list(reversed(held))
    for way in range(2):
        passing_meta(way, H).wait_recv()
        for p in range(plan.pieces[H]):
            passing(way, H, p).wait_recv()
    pick_all(H)
    flush(picked, hand_over)
    for d in range(H // 2):
        if d not in done:
            compute(d)
    compute(H - 1)
    flush(computed, give_back)
    for d in rest[:1]:
        land(d)
        flush(picked, hand_over)
    compute(H)
    for d in rest[1:2]:
        land(d)
    flush(computed, give_back)
    flush(picked, hand_over)
    for d in rest[:1]:
        compute(d)
        flush(computed, give_back)
    combine(H)
    for d in rest[2:]:
        land(d)
        flush(picked, hand_over)
    combine(H - 1)
    for i, d in enumerate(rest):
        for e in rest[i + 1 : i + 2]:
            compute(e)
            flush(computed, give_back)
        combine(d)
    for d in range(H // 2 - 1, 0, -1):
        combine(d)

    wait_rows(0)
    prepare(0, 0, 0)
    order = []
    for way in range(2):
        slot = iota((rows, rows), 0).astype(jnp.float32)
        rank = meta_ref[2, 4 + way : 5 + way, :]
        order.append(jnp.where(slot == rank, 1.0, 0.0).T.astype(jnp.bfloat16))

        def arrive(p, carry, way=way):
            closer(way, 1, p).wait_recv()
            return carry

        lax.fori_loop(0, plan.pieces[1], arrive, 0)
    squares = jnp.zeros((rows, 1), jnp.float32)
    first = plan.offset[1]
    sums = []
    for c in range(0, width, wide):
        part = jnp.dot(spread[0], doubled[0, :, c : c + wide], preferred_element_type=jnp.float32)
        for way in range(2):
            part = part + jnp.dot(
                order[way], back[way, first : first + rows, c : c + wide],
                preferred_element_type=jnp.float32,
            )
        sums.append(part)
        squares = squares + jnp.sum(part * part, axis=1, keepdims=True)
    inverse = lax.rsqrt(squares / width + EPS)
    half_width = width // 2
    here = min(wide, half_width)
    for i, c in enumerate(range(0, width, wide)):
        scaled = (sums[i] * inverse).astype(jnp.bfloat16)
        for s in range(0, wide, here):
            halves[(c + s) // half_width, :, (c + s) % half_width : (c + s) % half_width + here] = (
                scaled[:, s : s + here]
            )
    mine = pl.ds(pl.multiple_of(core * rows, rows), rows)
    swap = remote(halves.at[other], final.at[mine, :], fsem.at[0], fsem.at[1], tp=other)
    swap.start()
    final[mine, :] = halves[core]

    for j in range(Z):
        for r in range(1, X):
            hand_over(j, r).wait_send()
            give_back(j, r).wait_send()
    for d in range(1, H + 1):
        for way in range(2):
            passing_meta(way, d).wait_send()

            def gone(p, carry, way=way, d=d):
                closer(way, d, p).wait_send()
                return carry

            lax.fori_loop(0, plan.pieces[d], gone, 0)
    for p in range(plan.pieces[1]):
        for way in range(2):
            passing(way, 1, p).wait_send()
    theirs = pl.ds(pl.multiple_of(other * rows, rows), rows)
    swap.wait_send()
    remote(halves.at[core], final.at[theirs, :], fsem.at[0], fsem.at[1], tp=other).wait_recv()
    out_ref[...] = final[...]


def run_experts(plan, plus, minus, meta, w_gate, w_up, w_down):
    X, Z, H, rows, width = plan.X, plan.Z, plan.H, plan.rows, plan.width
    dma = pltpu.SemaphoreType.DMA
    hops = (2, H, plan.most)
    bf16 = jnp.bfloat16
    return pl.pallas_call(
        functools.partial(experts_kernel, plan),
        out_shape=jax.ShapeDtypeStruct((2 * rows, width // 2), bf16),
        in_specs=[VMEM, VMEM, VMEM, ANY, ANY, ANY],
        out_specs=VMEM,
        scratch_shapes=[
            pltpu.VMEM((2, plan.total, width), bf16),
            pltpu.VMEM((2, plan.total, width), bf16),
            pltpu.VMEM((2, H, 8, rows), jnp.float32),
            pltpu.VMEM((Z, plan.slots, width), bf16),
            pltpu.VMEM((Z, plan.slots, width), bf16),
            pltpu.VMEM((Z, plan.slots, width), bf16),
            pltpu.VMEM((2, rows, 2 * plan.slots), bf16),
            pltpu.VMEM((2, 2 * plan.slots, width), bf16),
            pltpu.VMEM((2,) + w_gate.shape, bf16),
            pltpu.VMEM((2,) + w_up.shape, bf16),
            pltpu.VMEM((2,) + w_down.shape, bf16),
            pltpu.VMEM((2, rows, width // 2), bf16),
            pltpu.VMEM((2 * rows, width // 2), bf16),
            dma(hops), dma(hops), dma(hops), dma(hops), dma((2, H)), dma((2, H)),
            dma((Z, X)), dma((Z, X)), dma((Z, X)), dma((Z, X)),
            dma((3,)), dma((3,)), dma((3,)), dma((2,)),
        ],
        compiler_params=pltpu.CompilerParams(
            collective_id=0, has_side_effects=True, vmem_limit_bytes=VMEM_LIMIT
        ),
        name="run_experts",
    )(plus, minus, meta, w_gate, w_up, w_down)


def per_device(columns, tokens, gain_in, expert_ids, gate_weights, w_gate, w_up, w_down, gain_out):
    own_rows, width = tokens.shape
    members = lax.axis_size("ep")
    capacity = 2 * own_rows * expert_ids.shape[1] // members
    plan = Plan(own_rows, width, members, capacity, columns)
    plus, minus, meta = sort_tokens(plan, tokens, gain_in, expert_ids, gate_weights)
    scaled = run_experts(plan, plus, minus, meta, w_gate[0], w_up[0], w_down[0])
    return (scaled.astype(jnp.float32) * gain_out).astype(jnp.bfloat16)


def solution(mesh, columns=COLUMNS):
    placed = (
        P(("grp", "ep", "tp"), None),
        P(),
        P(("grp", "ep"), None),
        P(("grp", "ep"), None),
        P("ep", None, "tp"),
        P("ep", None, "tp"),
        P("ep", None, "tp"),
        P("tp"),
    )
    return jax.shard_map(
        functools.partial(per_device, columns),
        mesh=mesh, in_specs=placed, out_specs=P(("grp", "ep"), "tp"), check_vma=False,
    )
```

time: 380 us -> 334 us (0.88)
  matrix products: 24.9 us -> 0 us
  blocking collectives: 11.6 us -> 0 us
  other arithmetic: 8.95 us -> 2.44 us
  local copies, waits for them, and re-layouts: 4.5 us -> 0.01 us
    dot_general x4 -> x0, matrix products: 24.9 us -> none  [the longest x2 18 us: expert_half(): lax.dot_general(hidden, down_matrix, (((1,), (1,)), ((), ())), preferred_...]
    all_to_all x1 -> x0, blocking collectives: 11.6 us -> none  [per_device(): lax.all_to_all(scaled, 'tp', split_axis=1, concat_axis=0, tiled=True)]
    convert_element_type x1 -> x0, other arithmetic: 7.74 us -> none  [per_device(): scaled = combine(plan, summed.astype(jnp.bfloat16), meta, metas)]
    pallas_call x2 -> x1, Pallas kernels: 325 us -> 326 us  [run_experts(): pl.pallas_call(functools.partial(experts_kernel, plan), out_shape=jax.Sha...]
where the time goes in v2:
time: 334 us
  Pallas kernels  331 us (99%)
    pallas_call x1, Pallas kernels, run_experts(): pl.pallas_call(functools.partial(experts_kernel, plan), out_shape=jax.Sha...  326 us

profile of v2, /device:TPU:33, one launch (start us, length us, event | category | flops | bytes accessed | tf_op | source)
XLA Modules:
  0.0 333.5 jit_solution(2769671040353981327)
XLA Ops:
  0.0 4.9 %sort_tokens.1 = (bf16[256,2048]{1,0:T(8,128)(2,1)}, bf16[256,2048]{1,0:T(8,128)(2,1)}, f32[3,8,256]{2,1,0:T(8,128)}) custom-call(bf16[256,2048]{1,0:T(8,128)(2,1)} %x_ref.1, f32[1,2048]{1,0:T(1,128)} %bitcast.9, s32[2,512]{1,0:T(2,128)} %bitcast.10, f32[2,512]{1,0:T(2,128)} %bitcast.11), custom_call_target="tpu_custom_call" | custom-call | tf_op jit(solution)/shard_map/sort_tokens/pallas_call | solution.py:132
  4.9 0.0 copy-start
  4.9 326.2 %run_experts.1 = bf16[512,1024]{1,0:T(8,128)(2,1)} custom-call(bf16[256,2048]{1,0:T(8,128)(2,1)} %get-tuple-element.8.plus_ref, bf16[256,2048]{1,0:T(8,128)(2,1)} %get-tuple-element.9.minus_ref, f32[3,8,256]{2,1,0:T(8,128)} %get-tuple-element.10.meta_ref, bf16[2048,256]{1,0:T(8,128)(2,1)} %bitcast.6, bf16[2048,256]{1,0:T(8,128)(2,1)} %bitcast.7, ...), custom_call_target="tpu_custom_call" | custom-call | tf_op jit(solution)/shard_map/run_experts/pallas_call | solution.py:492
  331.1 0.0 copy-done
  331.1 2.4 multiply_convert_fusion
Async XLA Ops:
  4.9 326.2 %copy-start = (f32[1024]{0:T(1024)S(1)}, f32[1024]{0:T(1024)}, u32[]{:S(2)}) copy-start(f32[1024]{0:T(1024)} %param.15) | copy-start | bytes 12292

commit v3 on v2

--- a/solution.py
+++ b/solution.py
@@ -44,23 +44,22 @@
     )
 
 
-def greet(plan, partner):
+def greet(plan):
     z, x = plan.me()
-    barrier = pltpu.get_barrier_semaphore()
     peers = [{"ep": plan.at(z + 1, x)}, {"ep": plan.at(z - 1, x)}]
     peers += [{"ep": plan.at(z, x + r)} for r in range(1, plan.X)]
-    if partner:
-        peers.append({"tp": 1 - lax.axis_index("tp")})
+    peers.append({"tp": 1 - lax.axis_index("tp")})
+    barrier = pltpu.get_barrier_semaphore()
     for peer in peers:
         pl.semaphore_signal(barrier, inc=1, device_id=peer, device_id_type=MESH)
-    pl.semaphore_wait(barrier, len(peers))
+    return barrier, len(peers)
 
 
 def iota(shape, dim):
     return lax.broadcasted_iota(jnp.int32, shape, dim)
 
 
-def sort_kernel(plan, x_ref, gain_ref, ids_ref, gates_ref, plus_ref, minus_ref, meta_ref, normed):
+def sort_tokens(plan, x_ref, gain_ref, ids_ref, gates_ref, plus_ref, minus_ref, meta_ref, normed):
     rows, X, Z, H = plan.rows, plan.X, plan.Z, plan.H
     z, _ = plan.me()
     step = 32
@@ -127,23 +126,6 @@
     meta_ref[2, 6:8, :] = jnp.zeros((2, rows), jnp.float32)
 
 
-def sort_tokens(plan, tokens, gain_in, expert_ids, gate_weights):
-    rows, width = plan.rows, plan.width
-    return pl.pallas_call(
-        functools.partial(sort_kernel, plan),
-        out_shape=(
-            jax.ShapeDtypeStruct((rows, width), jnp.bfloat16),
-            jax.ShapeDtypeStruct((rows, width), jnp.bfloat16),
-            jax.ShapeDtypeStruct((3, 8, rows), jnp.float32),
-        ),
-        in_specs=[VMEM] * 4,
-        out_specs=(VMEM,) * 3,
-        scratch_shapes=[pltpu.VMEM((rows, width), jnp.bfloat16)],
-        compiler_params=pltpu.CompilerParams(vmem_limit_bytes=VMEM_LIMIT),
-        name="sort_tokens",
-    )(tokens, gain_in.reshape(1, width), expert_ids.T, gate_weights.T)
-
-
 def hits(plan, meta, n, z, way, d, weighted):
     slots, cap = plan.slots, plan.cap
     slot = iota((slots, n), 0)
@@ -157,15 +139,41 @@
     return total
 
 
-def last_hop(plan, p):
-    return max(d for d in range(1, plan.H + 1) if plan.pieces[d] > p)
+def schedule(plan):
+    if plan.pieces != [0, 8, 8, 8, 8, 7, 5, 3, 1, 0]:
+        raise ValueError("no schedule")
+
+    def go(*pieces):
+        return [("go", d, p) for d, p in pieces]
+
+    def expert(d):
+        return [("expert", d, 0), ("expert", d, 1)]
+
+    def first(d):
+        return go((d, 0), (d, 1), (d, 2))
+
+    return (
+        first(1) + [("pick", 0)] + first(2) + first(3) + first(4) + [("expert", 0, 0)]
+        + first(5) + first(6) + first(7)
+        + go((1, 3), (8, 0), (1, 4), (1, 5)) + [("pick", 7)]
+        + go((2, 3), (2, 4), (1, 6)) + [("pick", 8)]
+        + go((3, 3), (3, 4), (2, 5)) + [("expert", 7, 0)]
+        + go((4, 3), (4, 4), (2, 6)) + [("expert", 7, 1)]
+        + go((5, 3), (5, 4), (3, 5)) + [("expert", 8, 0)]
+        + go((6, 3), (6, 4), (3, 6), (1, 7), (4, 5), (4, 6)) + [("pick", 6)]
+        + go((2, 7), (5, 5), (5, 6)) + expert(6)
+        + go((3, 7)) + [("sum", 8), ("pick", 5), ("sum", 7)]
+        + go((4, 7)) + expert(5) + [("sum", 6), ("pick", 4), ("pick", 3), ("sum", 5)]
+        + expert(4) + expert(3) + [("sum", 4), ("pick", 2), ("pick", 1)]
+        + expert(2) + [("sum", 3)] + expert(1) + [("sum", 2), ("sum", 1)]
+    )
 
 
 def experts_kernel(
     plan,
-    plus_ref, minus_ref, meta_ref, wg_ref, wu_ref, wd_ref,
+    x_ref, gain_ref, ids_ref, gates_ref, wg_ref, wu_ref, wd_ref,
     out_ref,
-    ring, back, metas, stage, arrived, rows_in, spread, doubled, wg, wu, wd, halves, final,
+    normed, plus_ref, minus_ref, meta_ref, ring, back, metas, stage, arrived, rows_in, spread, doubled, wg, wu, wd, halves, final,
     zsend, zrecv, bsend, brecv, msend, mrecv, xsend, xrecv, ysend, yrecv,
     wsend, wrecv, wown, fsem,
 ):
@@ -175,16 +183,13 @@
     z, x = plan.me()
     core = lax.axis_index("tp")
     other = 1 - core
-    greet(plan, True)
+    barrier, peers = greet(plan)
+    sort_tokens(plan, x_ref, gain_ref, ids_ref, gates_ref, plus_ref, minus_ref, meta_ref, normed)
+    pl.semaphore_wait(barrier, peers)
 
     own = (plus_ref, minus_ref)
     outward = (plan.at(z + 1, x), plan.at(z - 1, x))
     homeward = (outward[1], outward[0])
-    held = range(H // 2, H - 1)
-
-    def late(d, p):
-        return d in held and last_hop(plan, p) == d
-
     def places(d):
         if d == 0:
             return [(0, 0)]
@@ -225,17 +230,13 @@
         src, dst = arrived.at[j, column(r), :], rows_in.at[j, column(0), :]
         return remote(src, dst, ysend.at[j, r], yrecv.at[j, r], ep=plan.at(z, x + r))
 
-    picked, computed = [], []
-
-    def flush(waiting, copy):
-        for j in waiting:
-            for r in range(1, X):
-                copy(j, r).start()
-            if copy is hand_over:
-                arrived[j, column(0), :] = stage[j, column(0), :]
-            else:
-                rows_in[j, column(0), :] = arrived[j, column(0), :]
-        waiting.clear()
+    def exchange(j, copy):
+        for r in range(1, X):
+            copy(j, r).start()
+        if copy is hand_over:
+            arrived[j, column(0), :] = stage[j, column(0), :]
+        else:
+            rows_in[j, column(0), :] = arrived[j, column(0), :]
 
     def pick(way, d, j):
         n = rows if d == 0 else plan.prefix[d]
@@ -256,19 +257,37 @@
 
         lax.fori_loop(0, width // wide, columns, 0)
 
-    def pick_all(d):
+    landed = set()
+
+    def await_piece(d, p):
+        if (d, p) not in landed:
+            for way in range(2):
+                passing(way, d, p).wait_recv()
+            landed.add((d, p))
+
+    def pass_on(d, p):
+        for way in range(2):
+            if p == 0 and d > 1:
+                passing_meta(way, d - 1).wait_recv()
+            if p == 0:
+                passing_meta(way, d).start()
+        if d > 1:
+            await_piece(d - 1, p)
+        for way in range(2):
+            passing(way, d, p).start()
+
+    def pick_plane(d):
+        if d == H:
+            for way in range(2):
+                passing_meta(way, d).wait_recv()
+        for p in range(plan.pieces[d]):
+            await_piece(d, p)
         for way, j in places(d):
             pick(way, d, j)
-        picked.extend(spots(d))
-
-    def land(d):
-        for p in range(plan.pieces[d]):
-            if late(d, p):
-                for way in range(2):
-                    passing(way, d, p).wait_recv()
-        pick_all(d)
-
-    def expert(j, carry):
+        for j in spots(d):
+            exchange(j, hand_over)
+
+    def expert(j):
         hidden = []
         for half in range(2):
             gated = jnp.dot(arrived[j], wg[half], preferred_element_type=jnp.float32)
@@ -289,14 +308,13 @@
             return carry
 
         lax.fori_loop(0, width // step, down, 0)
-        return carry
-
-    def compute(d):
-        for j in spots(d):
-            for r in range(1, X):
-                hand_over(j, r).wait_recv()
-        lax.fori_loop(spots(d)[0], spots(d)[-1] + 1, expert, 0)
-        computed.extend(spots(d))
+
+    def compute(d, n):
+        j = spots(d)[n]
+        for r in range(1, X):
+            hand_over(j, r).wait_recv()
+        expert(j)
+        exchange(j, give_back)
 
     def prepare(way, d, j):
         n = rows if d == 0 else plan.prefix[d]
@@ -345,83 +363,25 @@
         if old:
             lax.fori_loop(0, old, functools.partial(one, joined=True), 0)
 
-    for way in range(2):
-        passing_meta(way, 1).start()
-    for p in range(plan.pieces[1]):
-        for way in range(2):
-            passing(way, 1, p).start()
     weights = []
     for i, (src, dst) in enumerate(((wg_ref, wg), (wu_ref, wu), (wd_ref, wd))):
         weights.append(remote(src, dst.at[1], wsend.at[i], wrecv.at[i], tp=other))
         weights.append(pltpu.make_async_copy(src, dst.at[0], wown.at[i]))
-    for copy in weights:
-        copy.start()
-    pick_all(0)
-    done = []
-    for d in range(1, H):
-        for way in range(2):
-            passing_meta(way, d).wait_recv()
-            passing_meta(way, d + 1).start()
-        for p in range(plan.pieces[d]):
-            if not late(d, p):
-                for way in range(2):
-                    passing(way, d, p).wait_recv()
-                    if p < plan.pieces[d + 1] and not late(d + 1, p):
-                        passing(way, d + 1, p).start()
-        flush(picked, hand_over)
-        flush(computed, give_back)
-        if d == H - 1:
-            for e in reversed(held):
-                for p in range(plan.pieces[e]):
-                    if late(e, p):
-                        for way in range(2):
-                            passing(way, e, p).start()
-        if d not in held:
-            pick_all(d)
-        if d == 1:
+    for i, (kind, d, *which) in enumerate(schedule(plan)):
+        if kind == "go":
+            pass_on(d, *which)
+        elif kind == "pick":
+            pick_plane(d)
+        elif kind == "expert":
+            if d == 0:
+                for copy in weights:
+                    copy.wait()
+            compute(d, *which)
+        else:
+            combine(d)
+        if i == 2:
             for copy in weights:
-                copy.wait()
-        if 0 <= d - 2 < H // 2:
-            compute(d - 2)
-            done.append(d - 2)
-    flush(picked, hand_over)
-    flush(computed, give_back)
-
-    rest = list(reversed(held))
-    for way in range(2):
-        passing_meta(way, H).wait_recv()
-        for p in range(plan.pieces[H]):
-            passing(way, H, p).wait_recv()
-    pick_all(H)
-    flush(picked, hand_over)
-    for d in range(H // 2):
-        if d not in done:
-            compute(d)
-    compute(H - 1)
-    flush(computed, give_back)
-    for d in rest[:1]:
-        land(d)
-        flush(picked, hand_over)
-    compute(H)
-    for d in rest[1:2]:
-        land(d)
-    flush(computed, give_back)
-    flush(picked, hand_over)
-    for d in rest[:1]:
-        compute(d)
-        flush(computed, give_back)
-    combine(H)
-    for d in rest[2:]:
-        land(d)
-        flush(picked, hand_over)
-    combine(H - 1)
-    for i, d in enumerate(rest):
-        for e in rest[i + 1 : i + 2]:
-            compute(e)
-            flush(computed, give_back)
-        combine(d)
-    for d in range(H // 2 - 1, 0, -1):
-        combine(d)
+                copy.start()
 
     wait_rows(0)
     prepare(0, 0, 0)
@@ -484,7 +444,7 @@
     out_ref[...] = final[...]
 
 
-def run_experts(plan, plus, minus, meta, w_gate, w_up, w_down):
+def run_experts(plan, tokens, gain_in, expert_ids, gate_weights, w_gate, w_up, w_down):
     X, Z, H, rows, width = plan.X, plan.Z, plan.H, plan.rows, plan.width
     dma = pltpu.SemaphoreType.DMA
     hops = (2, H, plan.most)
@@ -492,9 +452,13 @@
     return pl.pallas_call(
         functools.partial(experts_kernel, plan),
         out_shape=jax.ShapeDtypeStruct((2 * rows, width // 2), bf16),
-        in_specs=[VMEM, VMEM, VMEM, ANY, ANY, ANY],
+        in_specs=[VMEM, VMEM, VMEM, VMEM, ANY, ANY, ANY],
         out_specs=VMEM,
         scratch_shapes=[
+            pltpu.VMEM((rows, width), bf16),
+            pltpu.VMEM((rows, width), bf16),
+            pltpu.VMEM((rows, width), bf16),
+            pltpu.VMEM((3, 8, rows), jnp.float32),
             pltpu.VMEM((2, plan.total, width), bf16),
             pltpu.VMEM((2, plan.total, width), bf16),
             pltpu.VMEM((2, H, 8, rows), jnp.float32),
@@ -516,7 +480,7 @@
             collective_id=0, has_side_effects=True, vmem_limit_bytes=VMEM_LIMIT
         ),
         name="run_experts",
-    )(plus, minus, meta, w_gate, w_up, w_down)
+    )(tokens, gain_in.reshape(1, width), expert_ids.T, gate_weights.T, w_gate, w_up, w_down)
 
 
 def per_device(columns, tokens, gain_in, expert_ids, gate_weights, w_gate, w_up, w_down, gain_out):
@@ -524,8 +488,9 @@
     members = lax.axis_size("ep")
     capacity = 2 * own_rows * expert_ids.shape[1] // members
     plan = Plan(own_rows, width, members, capacity, columns)
-    plus, minus, meta = sort_tokens(plan, tokens, gain_in, expert_ids, gate_weights)
-    scaled = run_experts(plan, plus, minus, meta, w_gate[0], w_up[0], w_down[0])
+    scaled = run_experts(
+        plan, tokens, gain_in, expert_ids, gate_weights, w_gate[0], w_up[0], w_down[0]
+    )
     return (scaled.astype(jnp.float32) * gain_out).astype(jnp.bfloat16)
 
 

time: 334 us -> 313 us (0.937)
  Pallas kernels: 331 us -> 311 us
    pallas_call x1, Pallas kernels: 326 us -> 311 us  [run_experts(): pl.pallas_call(functools.partial(experts_kernel, plan), out_shape=jax.Sha...]
    pallas_call x1 -> x0, Pallas kernels: 4.89 us -> none  [sort_tokens(): pl.pallas_call(functools.partial(sort_kernel, plan), out_shape=(jax.Shape...]
where the time goes in v3:
time: 313 us
  Pallas kernels  311 us (99%)
    pallas_call x1, Pallas kernels, run_experts(): pl.pallas_call(functools.partial(experts_kernel, plan), out_shape=jax.Sha...  311 us

profile of v3, /device:TPU:33, one launch (start us, length us, event | category | flops | bytes accessed | tf_op | source)
XLA Modules:
  0.0 313.2 jit_solution(7281168402897279890)
XLA Ops:
  0.0 0.0 copy-start
  0.0 310.7 %run_experts.1 = bf16[512,1024]{1,0:T(8,128)(2,1)} custom-call(bf16[256,2048]{1,0:T(8,128)(2,1)} %x_ref.1, f32[1,2048]{1,0:T(1,128)} %bitcast.9, s32[2,512]{1,0:T(2,128)} %bitcast.10, f32[2,512]{1,0:T(2,128)} %bitcast.11, bf16[2048,256]{1,0:T(8,128)(2,1)} %bitcast.6, bf16[2048,256]{1,0:T(8,128)(2,1)} %bitcast.7, bf16[2048,256]{1,0:T(8,128)(2,1)} %bitcast.8), custom_call_target="tpu_custom_call" | custom-call | tf_op jit(solution)/shard_map/run_experts/pallas_call | solution.py:452
  310.7 0.0 copy-done
  310.7 2.4 multiply_convert_fusion
Async XLA Ops:
  0.0 310.7 %copy-start = (f32[1024]{0:T(1024)S(1)}, f32[1024]{0:T(1024)}, u32[]{:S(2)}) copy-start(f32[1024]{0:T(1024)} %param.15) | copy-start | bytes 12292

commit v4 on v3

--- a/solution.py
+++ b/solution.py
@@ -29,6 +29,9 @@
         self.offset = [sum(self.prefix[:d]) for d in range(self.H + 2)]
         self.total = sum(self.prefix)
         self.most = max(self.pieces)
+
+    def number(self, d, p):
+        return self.offset[d] // self.piece + p
 
     def me(self):
         ep = lax.axis_index("ep")
@@ -171,9 +174,10 @@
 
 def experts_kernel(
     plan,
-    x_ref, gain_ref, ids_ref, gates_ref, wg_ref, wu_ref, wd_ref,
+    x_ref, gain_ref, ids_ref, gates_ref, wg_ref, wu_ref, wd_ref, gain_out_ref,
     out_ref,
-    normed, plus_ref, minus_ref, meta_ref, ring, back, metas, stage, arrived, rows_in, spread, doubled, wg, wu, wd, halves, final,
+    normed, plus_ref, minus_ref, meta_ref, ring, back, metas, stage, arrived, rows_in, spread, doubled,
+    wg, wu, wd, halves, final,
     zsend, zrecv, bsend, brecv, msend, mrecv, xsend, xrecv, ysend, yrecv,
     wsend, wrecv, wown, fsem,
 ):
@@ -206,17 +210,17 @@
             src = own[way].at[pl.ds(p * piece, piece), :]
         else:
             src = ring.at[way, pl.ds(plan.offset[d - 1] + p * piece, piece), :]
-        return remote(src, dst, zsend.at[way, d - 1, p], zrecv.at[way, d - 1, p], ep=outward[way])
+        return remote(src, dst, zsend.at[way, d - 1], zrecv.at[way, plan.number(d, p)], ep=outward[way])
 
     def passing_meta(way, d):
         src = meta_ref.at[way] if d == 1 else metas.at[way, d - 2]
-        return remote(src, metas.at[way, d - 1], msend.at[way, d - 1], mrecv.at[way, d - 1], ep=outward[way])
+        return remote(src, metas.at[way, d - 1], msend.at[0], mrecv.at[way, d - 1], ep=outward[way])
 
     def closer(way, d, p):
         here = pl.ds(plan.offset[d] + p * piece, piece)
         return remote(
             ring.at[way, here, :], back.at[way, here, :],
-            bsend.at[way, d - 1, p], brecv.at[way, d - 1, p], ep=homeward[way],
+            bsend.at[way], brecv.at[way, plan.number(d, p)], ep=homeward[way],
         )
 
     def column(r):
@@ -224,11 +228,15 @@
 
     def hand_over(j, r):
         src, dst = stage.at[j, column(r), :], arrived.at[j, column(0), :]
-        return remote(src, dst, xsend.at[j, r], xrecv.at[j, r], ep=plan.at(z, x + r))
+        return remote(src, dst, xsend.at[0], xrecv.at[j], ep=plan.at(z, x + r))
 
     def give_back(j, r):
         src, dst = arrived.at[j, column(r), :], rows_in.at[j, column(0), :]
-        return remote(src, dst, ysend.at[j, r], yrecv.at[j, r], ep=plan.at(z, x + r))
+        return remote(src, dst, ysend.at[0], yrecv.at[j], ep=plan.at(z, x + r))
+
+    def all_columns(j, ref, send, recv):
+        part = ref.at[j, pl.ds(0, plan.slots - cap), :]
+        return remote(part, part, send, recv, ep=plan.at(z, x + 1))
 
     def exchange(j, copy):
         for r in range(1, X):
@@ -311,8 +319,7 @@
 
     def compute(d, n):
         j = spots(d)[n]
-        for r in range(1, X):
-            hand_over(j, r).wait_recv()
+        all_columns(j, arrived, xsend.at[0], xrecv.at[j]).wait_recv()
         expert(j)
         exchange(j, give_back)
 
@@ -327,8 +334,11 @@
 
     def wait_rows(d):
         for j in spots(d):
-            for r in range(1, X):
-                give_back(j, r).wait_recv()
+            all_columns(j, rows_in, ysend.at[0], yrecv.at[j]).wait_recv()
+
+    def hop_sent(way, d):
+        here = ring.at[way, pl.ds(plan.offset[d], plan.prefix[d]), :]
+        remote(here, here, zsend.at[way, d - 1], zrecv.at[way, 0], ep=outward[way]).wait_send()
 
     def combine(d):
         wait_rows(d)
@@ -336,8 +346,7 @@
             prepare(way, d, j)
         if d < H:
             for way in range(2):
-                for p in range(plan.pieces[d + 1]):
-                    passing(way, d + 1, p).wait_send()
+                hop_sent(way, d + 1)
 
         def one(p, carry, joined):
             for way in range(2):
@@ -422,37 +431,30 @@
     swap.start()
     final[mine, :] = halves[core]
 
-    for j in range(Z):
-        for r in range(1, X):
-            hand_over(j, r).wait_send()
-            give_back(j, r).wait_send()
-    for d in range(1, H + 1):
-        for way in range(2):
-            passing_meta(way, d).wait_send()
-
-            def gone(p, carry, way=way, d=d):
-                closer(way, d, p).wait_send()
-                return carry
-
-            lax.fori_loop(0, plan.pieces[d], gone, 0)
-    for p in range(plan.pieces[1]):
-        for way in range(2):
-            passing(way, 1, p).wait_send()
+    sent = pl.ds(0, Z * (X - 1) // X)
+    remote(stage.at[sent], stage.at[sent], xsend.at[0], xrecv.at[0], ep=outward[0]).wait_send()
+    remote(arrived.at[sent], arrived.at[sent], ysend.at[0], yrecv.at[0], ep=outward[0]).wait_send()
+    remote(metas, metas, msend.at[0], mrecv.at[0, 0], ep=outward[0]).wait_send()
+    for way in range(2):
+        hop_sent(way, 1)
+        remote(
+            ring.at[way], ring.at[way], bsend.at[way], brecv.at[way, 0], ep=homeward[way]
+        ).wait_send()
     theirs = pl.ds(pl.multiple_of(other * rows, rows), rows)
     swap.wait_send()
     remote(halves.at[core], final.at[theirs, :], fsem.at[0], fsem.at[1], tp=other).wait_recv()
-    out_ref[...] = final[...]
-
-
-def run_experts(plan, tokens, gain_in, expert_ids, gate_weights, w_gate, w_up, w_down):
+    out_ref[...] = (final[...].astype(jnp.float32) * gain_out_ref[...]).astype(jnp.bfloat16)
+
+
+def run_experts(plan, tokens, gain_in, expert_ids, gate_weights, w_gate, w_up, w_down, gain_out):
     X, Z, H, rows, width = plan.X, plan.Z, plan.H, plan.rows, plan.width
     dma = pltpu.SemaphoreType.DMA
-    hops = (2, H, plan.most)
+    hops = (2, sum(plan.pieces))
     bf16 = jnp.bfloat16
     return pl.pallas_call(
         functools.partial(experts_kernel, plan),
         out_shape=jax.ShapeDtypeStruct((2 * rows, width // 2), bf16),
-        in_specs=[VMEM, VMEM, VMEM, VMEM, ANY, ANY, ANY],
+        in_specs=[VMEM, VMEM, VMEM, VMEM, ANY, ANY, ANY, VMEM],
         out_specs=VMEM,
         scratch_shapes=[
             pltpu.VMEM((rows, width), bf16),
@@ -472,15 +474,18 @@
             pltpu.VMEM((2,) + w_down.shape, bf16),
             pltpu.VMEM((2, rows, width // 2), bf16),
             pltpu.VMEM((2 * rows, width // 2), bf16),
-            dma(hops), dma(hops), dma(hops), dma(hops), dma((2, H)), dma((2, H)),
-            dma((Z, X)), dma((Z, X)), dma((Z, X)), dma((Z, X)),
+            dma((2, H)), dma(hops), dma((2,)), dma(hops), dma((1,)), dma((2, H)),
+            dma((1,)), dma((Z,)), dma((1,)), dma((Z,)),
             dma((3,)), dma((3,)), dma((3,)), dma((2,)),
         ],
         compiler_params=pltpu.CompilerParams(
             collective_id=0, has_side_effects=True, vmem_limit_bytes=VMEM_LIMIT
         ),
         name="run_experts",
-    )(tokens, gain_in.reshape(1, width), expert_ids.T, gate_weights.T, w_gate, w_up, w_down)
+    )(
+        tokens, gain_in.reshape(1, width), expert_ids.T, gate_weights.T,
+        w_gate, w_up, w_down, gain_out.reshape(1, width // 2),
+    )
 
 
 def per_device(columns, tokens, gain_in, expert_ids, gate_weights, w_gate, w_up, w_down, gain_out):
@@ -488,10 +493,9 @@
     members = lax.axis_size("ep")
     capacity = 2 * own_rows * expert_ids.shape[1] // members
     plan = Plan(own_rows, width, members, capacity, columns)
-    scaled = run_experts(
-        plan, tokens, gain_in, expert_ids, gate_weights, w_gate[0], w_up[0], w_down[0]
+    return run_experts(
+        plan, tokens, gain_in, expert_ids, gate_weights, w_gate[0], w_up[0], w_down[0], gain_out
     )
-    return (scaled.astype(jnp.float32) * gain_out).astype(jnp.bfloat16)
 
 
 def solution(mesh, columns=COLUMNS):

time: 313 us -> 308 us (0.984)
  Pallas kernels: 311 us -> 306 us
    pallas_call x1, Pallas kernels: 311 us -> 306 us  [run_experts(): pl.pallas_call(functools.partial(experts_kernel, plan), out_shape=jax.Sha...]
where the time goes in v4:
time: 308 us
  Pallas kernels  306 us (99%)
    pallas_call x1, Pallas kernels, run_experts(): pl.pallas_call(functools.partial(experts_kernel, plan), out_shape=jax.Sha...  306 us

profile of v4, /device:TPU:33, one launch (start us, length us, event | category | flops | bytes accessed | tf_op | source)
XLA Modules:
  0.0 308.3 jit_solution(14122543842450258947)
XLA Ops:
  0.0 306.0 %run_experts.1 = bf16[512,1024]{1,0:T(8,128)(2,1)} custom-call(bf16[256,2048]{1,0:T(8,128)(2,1)} %x_ref.1, f32[1,2048]{1,0:T(1,128)} %bitcast.10, s32[2,512]{1,0:T(2,128)} %bitcast.11, f32[2,512]{1,0:T(2,128)} %bitcast.12, bf16[2048,256]{1,0:T(8,128)(2,1)} %bitcast.7, bf16[2048,256]{1,0:T(8,128)(2,1)} %bitcast.8, bf16[2048,256]{1,0:T(8,128)(2,1)} %bitcast.9, ...), custom_call_target="tpu_custom_call" | custom-call | tf_op jit(solution)/shard_map/run_experts/pallas_call | solution.py:454
  306.0 2.3 copy.10

commit v5 on v4

--- a/solution.py
+++ b/solution.py
@@ -62,7 +62,7 @@
     return lax.broadcasted_iota(jnp.int32, shape, dim)
 
 
-def sort_tokens(plan, x_ref, gain_ref, ids_ref, gates_ref, plus_ref, minus_ref, meta_ref, normed):
+def sort_tokens(plan, x_ref, gain_ref, ids_ref, gates_ref, own, orders, meta_ref, normed):
     rows, X, Z, H = plan.rows, plan.X, plan.Z, plan.H
     z, _ = plan.me()
     step = 32
@@ -76,7 +76,7 @@
 
     lax.fori_loop(0, rows // step, norm_step, 0)
 
-    own = pl.ds(pl.multiple_of(lax.axis_index("tp") * rows, rows), rows)
+    mine = pl.ds(pl.multiple_of(lax.axis_index("tp") * rows, rows), rows)
     square = (rows, rows)
     sub, lane = iota(square, 0), iota(square, 1)
     eye = sub == lane
@@ -87,9 +87,9 @@
     def count(mask, axis):
         return jnp.sum(jnp.where(mask, 1.0, 0.0), axis=axis, keepdims=True)
 
-    rws = [ids_ref[k : k + 1, own].astype(jnp.float32) for k in range(2)]
+    rws = [ids_ref[k : k + 1, mine].astype(jnp.float32) for k in range(2)]
     cols = [as_column(r) for r in rws]
-    grws = [gates_ref[k : k + 1, own] for k in range(2)]
+    grws = [gates_ref[k : k + 1, mine] for k in range(2)]
     gcols = [as_column(g) for g in grws]
     q_col, q_row, key_col, key_row = [], [], [[], []], [[], []]
     for k in range(2):
@@ -109,7 +109,7 @@
     for k in range(2):
         meta_ref[2, k : k + 1, :] = q_row[k]
         meta_ref[2, 2 + k : 3 + k, :] = grws[k]
-    for way, out in ((0, plus_ref), (1, minus_ref)):
+    for way in range(2):
         far_col = jnp.maximum(*key_col[way])
         far_row = jnp.maximum(*key_row[way])
         rank_row = count((far_col > far_row) | ((far_col == far_row) & (sub < lane)), 0)
@@ -120,13 +120,18 @@
             meta_ref[way, k : k + 1, :] = jnp.sum(jnp.where(chosen, q_col[k], 0.0), axis=0, keepdims=True)
             meta_ref[way, 2 + k : 3 + k, :] = jnp.sum(jnp.where(chosen, gcols[k], 0.0), axis=0, keepdims=True)
         meta_ref[way, 4:8, :] = jnp.zeros((4, rows), jnp.float32)
-        order = jnp.where(sub.astype(jnp.float32) == rank_row, 1.0, 0.0).astype(jnp.bfloat16)
-        for c in range(0, plan.width, 512):
-            n = min(512, plan.width)
-            out[:, c : c + n] = jnp.dot(
-                order, normed[:, c : c + n], preferred_element_type=jnp.float32
-            ).astype(jnp.bfloat16)
+        orders[way] = jnp.where(sub.astype(jnp.float32) == rank_row, 1.0, 0.0).astype(jnp.bfloat16)
     meta_ref[2, 6:8, :] = jnp.zeros((2, rows), jnp.float32)
+
+    def write(lo, hi):
+        n = min(512, plan.width)
+        for way in range(2):
+            for c in range(0, plan.width, n):
+                own[way][lo:hi, c : c + n] = jnp.dot(
+                    orders[way, lo:hi, :], normed[:, c : c + n], preferred_element_type=jnp.float32
+                ).astype(jnp.bfloat16)
+
+    return write
 
 
 def hits(plan, meta, n, z, way, d, weighted):
@@ -177,9 +182,9 @@
     x_ref, gain_ref, ids_ref, gates_ref, wg_ref, wu_ref, wd_ref, gain_out_ref,
     out_ref,
     normed, plus_ref, minus_ref, meta_ref, ring, back, metas, stage, arrived, rows_in, spread, doubled,
-    wg, wu, wd, halves, final,
+    wg, wu, wd, halves, final, orders, unsort, gathered,
     zsend, zrecv, bsend, brecv, msend, mrecv, xsend, xrecv, ysend, yrecv,
-    wsend, wrecv, wown, fsem,
+    wsend, wrecv, wown, fsend, frecv, osem,
 ):
     X, Z, H, cap, piece = plan.X, plan.Z, plan.H, plan.cap, plan.piece
     rows, width, slots = plan.rows, plan.width, plan.slots
@@ -188,10 +193,12 @@
     core = lax.axis_index("tp")
     other = 1 - core
     barrier, peers = greet(plan)
-    sort_tokens(plan, x_ref, gain_ref, ids_ref, gates_ref, plus_ref, minus_ref, meta_ref, normed)
+    own = (plus_ref, minus_ref)
+    write = sort_tokens(plan, x_ref, gain_ref, ids_ref, gates_ref, own, orders, meta_ref, normed)
+    lead = 3 * piece
+    write(0, lead)
     pl.semaphore_wait(barrier, peers)
 
-    own = (plus_ref, minus_ref)
     outward = (plan.at(z + 1, x), plan.at(z - 1, x))
     homeward = (outward[1], outward[0])
     def places(d):
@@ -372,6 +379,18 @@
         if old:
             lax.fori_loop(0, old, functools.partial(one, joined=True), 0)
 
+    def own_rows():
+        wait_rows(0)
+        prepare(0, 0, 0)
+        for c in range(0, width, wide):
+            gathered[:, c : c + wide] = jnp.dot(
+                spread[0], doubled[0, :, c : c + wide], preferred_element_type=jnp.float32
+            )
+        for way in range(2):
+            slot = iota((rows, rows), 0).astype(jnp.float32)
+            rank = meta_ref[2, 4 + way : 5 + way, :]
+            unsort[way] = jnp.where(slot == rank, 1.0, 0.0).T.astype(jnp.bfloat16)
+
     weights = []
     for i, (src, dst) in enumerate(((wg_ref, wg), (wu_ref, wu), (wd_ref, wd))):
         weights.append(remote(src, dst.at[1], wsend.at[i], wrecv.at[i], tp=other))
@@ -387,49 +406,70 @@
                     copy.wait()
             compute(d, *which)
         else:
+            if d == 1:
+                own_rows()
             combine(d)
         if i == 2:
+            write(lead, rows)
             for copy in weights:
                 copy.start()
 
-    wait_rows(0)
-    prepare(0, 0, 0)
-    order = []
+    first, end = plan.offset[1], plan.offset[1] + rows
+    early = end - piece
     for way in range(2):
-        slot = iota((rows, rows), 0).astype(jnp.float32)
-        rank = meta_ref[2, 4 + way : 5 + way, :]
-        order.append(jnp.where(slot == rank, 1.0, 0.0).T.astype(jnp.bfloat16))
-
         def arrive(p, carry, way=way):
             closer(way, 1, p).wait_recv()
             return carry
 
-        lax.fori_loop(0, plan.pieces[1], arrive, 0)
-    squares = jnp.zeros((rows, 1), jnp.float32)
-    first = plan.offset[1]
-    sums = []
+        lax.fori_loop(0, plan.pieces[1] - 1, arrive, 0)
     for c in range(0, width, wide):
-        part = jnp.dot(spread[0], doubled[0, :, c : c + wide], preferred_element_type=jnp.float32)
+        part = gathered[:, c : c + wide]
         for way in range(2):
             part = part + jnp.dot(
-                order[way], back[way, first : first + rows, c : c + wide],
+                unsort[way, :, : rows - piece], back[way, first:early, c : c + wide],
                 preferred_element_type=jnp.float32,
             )
-        sums.append(part)
-        squares = squares + jnp.sum(part * part, axis=1, keepdims=True)
-    inverse = lax.rsqrt(squares / width + EPS)
-    half_width = width // 2
+        gathered[:, c : c + wide] = part
+    for way in range(2):
+        closer(way, 1, plan.pieces[1] - 1).wait_recv()
+    gain = gain_out_ref[...]
+    half_width, some = width // 2, rows // 2
     here = min(wide, half_width)
-    for i, c in enumerate(range(0, width, wide)):
-        scaled = (sums[i] * inverse).astype(jnp.bfloat16)
-        for s in range(0, wide, here):
-            halves[(c + s) // half_width, :, (c + s) % half_width : (c + s) % half_width + here] = (
-                scaled[:, s : s + here]
-            )
-    mine = pl.ds(pl.multiple_of(core * rows, rows), rows)
-    swap = remote(halves.at[other], final.at[mine, :], fsem.at[0], fsem.at[1], tp=other)
-    swap.start()
-    final[mine, :] = halves[core]
+
+    def swap(i):
+        src = halves.at[other, pl.ds(i * some, some), :]
+        return remote(src, final.at[1, pl.ds(i * some, some), :], fsend.at[i], frecv.at[i], tp=other)
+
+    def put(i, who):
+        at = pl.ds(pl.multiple_of((core if who == 0 else other) * rows + i * some, some), some)
+        return pltpu.make_async_copy(
+            final.at[2 * who, pl.ds(i * some, some), :], out_ref.at[at, :], osem.at[who, i]
+        )
+
+    for i in range(2):
+        part_rows = slice(i * some, (i + 1) * some)
+        squares = jnp.zeros((some, 1), jnp.float32)
+        for c in range(0, width, wide):
+            part = gathered[part_rows, c : c + wide]
+            for way in range(2):
+                part = part + jnp.dot(
+                    unsort[way, part_rows, rows - piece :], back[way, early:end, c : c + wide],
+                    preferred_element_type=jnp.float32,
+                )
+            gathered[part_rows, c : c + wide] = part
+            squares = squares + jnp.sum(part * part, axis=1, keepdims=True)
+        inverse = lax.rsqrt(squares / width + EPS)
+        for c in range(0, width, here):
+            halves[c // half_width, part_rows, c % half_width : c % half_width + here] = (
+                gathered[part_rows, c : c + here] * inverse
+            ).astype(jnp.bfloat16)
+        swap(i).start()
+    for i in range(2):
+        part_rows = slice(i * some, (i + 1) * some)
+        final[0, part_rows, :] = (
+            halves[core, part_rows, :].astype(jnp.float32) * gain
+        ).astype(jnp.bfloat16)
+        put(i, 0).start()
 
     sent = pl.ds(0, Z * (X - 1) // X)
     remote(stage.at[sent], stage.at[sent], xsend.at[0], xrecv.at[0], ep=outward[0]).wait_send()
@@ -440,10 +480,17 @@
         remote(
             ring.at[way], ring.at[way], bsend.at[way], brecv.at[way, 0], ep=homeward[way]
         ).wait_send()
-    theirs = pl.ds(pl.multiple_of(other * rows, rows), rows)
-    swap.wait_send()
-    remote(halves.at[core], final.at[theirs, :], fsem.at[0], fsem.at[1], tp=other).wait_recv()
-    out_ref[...] = (final[...].astype(jnp.float32) * gain_out_ref[...]).astype(jnp.bfloat16)
+    for i in range(2):
+        part_rows = slice(i * some, (i + 1) * some)
+        swap(i).wait_recv()
+        final[2, part_rows, :] = (
+            final[1, part_rows, :].astype(jnp.float32) * gain
+        ).astype(jnp.bfloat16)
+        put(i, 1).start()
+    for i in range(2):
+        swap(i).wait_send()
+        for who in range(2):
+            put(i, who).wait()
 
 
 def run_experts(plan, tokens, gain_in, expert_ids, gate_weights, w_gate, w_up, w_down, gain_out):
@@ -455,7 +502,7 @@
         functools.partial(experts_kernel, plan),
         out_shape=jax.ShapeDtypeStruct((2 * rows, width // 2), bf16),
         in_specs=[VMEM, VMEM, VMEM, VMEM, ANY, ANY, ANY, VMEM],
-        out_specs=VMEM,
+        out_specs=ANY,
         scratch_shapes=[
             pltpu.VMEM((rows, width), bf16),
             pltpu.VMEM((rows, width), bf16),
@@ -473,10 +520,13 @@
             pltpu.VMEM((2,) + w_up.shape, bf16),
             pltpu.VMEM((2,) + w_down.shape, bf16),
             pltpu.VMEM((2, rows, width // 2), bf16),
-            pltpu.VMEM((2 * rows, width // 2), bf16),
+            pltpu.VMEM((3, rows, width // 2), bf16),
+            pltpu.VMEM((2, rows, rows), bf16),
+            pltpu.VMEM((2, rows, rows), bf16),
+            pltpu.VMEM((rows, width), jnp.float32),
             dma((2, H)), dma(hops), dma((2,)), dma(hops), dma((1,)), dma((2, H)),
             dma((1,)), dma((Z,)), dma((1,)), dma((Z,)),
-            dma((3,)), dma((3,)), dma((3,)), dma((2,)),
+            dma((3,)), dma((3,)), dma((3,)), dma((2,)), dma((2,)), dma((2, 2)),
         ],
         compiler_params=pltpu.CompilerParams(
             collective_id=0, has_side_effects=True, vmem_limit_bytes=VMEM_LIMIT

time: 308 us -> 308 us (level)
  no operation moved by 1% of the time
where the time goes in v5:
time: 308 us
  Pallas kernels  305 us (99%)
    pallas_call x1, Pallas kernels, run_experts(): pl.pallas_call(functools.partial(experts_kernel, plan), out_shape=jax.Sha...  305 us

profile of v5, /device:TPU:33, one launch (start us, length us, event | category | flops | bytes accessed | tf_op | source)
XLA Modules:
  0.0 307.6 jit_solution(13647231592428671827)
XLA Ops:
  0.0 305.3 %run_experts.1 = bf16[512,1024]{1,0:T(8,128)(2,1)} custom-call(bf16[256,2048]{1,0:T(8,128)(2,1)} %x_ref.1, f32[1,2048]{1,0:T(1,128)} %bitcast.10, s32[2,512]{1,0:T(2,128)} %bitcast.11, f32[2,512]{1,0:T(2,128)} %bitcast.12, bf16[2048,256]{1,0:T(8,128)(2,1)} %bitcast.7, bf16[2048,256]{1,0:T(8,128)(2,1)} %bitcast.8, bf16[2048,256]{1,0:T(8,128)(2,1)} %bitcast.9, ...), custom_call_target="tpu_custom_call" | custom-call | tf_op jit(solution)/shard_map/run_experts/pallas_call | solution.py:501
  305.3 2.3 copy.10

commit v6 on v5

--- a/solution.py
+++ b/solution.py
@@ -179,11 +179,11 @@
 
 def experts_kernel(
     plan,
-    x_ref, gain_ref, ids_ref, gates_ref, wg_ref, wu_ref, wd_ref, gain_out_ref,
+    x_ref, gain_ref, ids_ref, gates_ref, wg_ref, wu_ref, wd_ref,
     out_ref,
     normed, plus_ref, minus_ref, meta_ref, ring, back, metas, stage, arrived, rows_in, spread, doubled,
-    wg, wu, wd, halves, final, orders, unsort, gathered,
-    zsend, zrecv, bsend, brecv, msend, mrecv, xsend, xrecv, ysend, yrecv,
+    wg, wu, wd, halves, orders, unsort, gathered,
+    zsend, zrecv, bsend, msend, mrecv, xsend, xrecv, ysend, yrecv,
     wsend, wrecv, wown, fsend, frecv, osem,
 ):
     X, Z, H, cap, piece = plan.X, plan.Z, plan.H, plan.cap, plan.piece
@@ -223,11 +223,14 @@
         src = meta_ref.at[way] if d == 1 else metas.at[way, d - 2]
         return remote(src, metas.at[way, d - 1], msend.at[0], mrecv.at[way, d - 1], ep=outward[way])
 
+    def back_sem(way, d, p):
+        return zrecv.at[way, plan.number(d - 1, p) if d > 1 else sum(plan.pieces) + p]
+
     def closer(way, d, p):
         here = pl.ds(plan.offset[d] + p * piece, piece)
         return remote(
             ring.at[way, here, :], back.at[way, here, :],
-            bsend.at[way], brecv.at[way, plan.number(d, p)], ep=homeward[way],
+            bsend.at[way], back_sem(way, d, p), ep=homeward[way],
         )
 
     def column(r):
@@ -432,19 +435,18 @@
         gathered[:, c : c + wide] = part
     for way in range(2):
         closer(way, 1, plan.pieces[1] - 1).wait_recv()
-    gain = gain_out_ref[...]
     half_width, some = width // 2, rows // 2
     here = min(wide, half_width)
 
-    def swap(i):
+    def block(of, i):
+        return out_ref.at[pl.ds(pl.multiple_of(of * rows + i * some, some), some), :]
+
+    def swap(i, of):
         src = halves.at[other, pl.ds(i * some, some), :]
-        return remote(src, final.at[1, pl.ds(i * some, some), :], fsend.at[i], frecv.at[i], tp=other)
-
-    def put(i, who):
-        at = pl.ds(pl.multiple_of((core if who == 0 else other) * rows + i * some, some), some)
-        return pltpu.make_async_copy(
-            final.at[2 * who, pl.ds(i * some, some), :], out_ref.at[at, :], osem.at[who, i]
-        )
+        return remote(src, block(of, i), fsend.at[i], frecv.at[i], tp=other)
+
+    def put(i):
+        return pltpu.make_async_copy(halves.at[core, pl.ds(i * some, some), :], block(core, i), osem.at[i])
 
     for i in range(2):
         part_rows = slice(i * some, (i + 1) * some)
@@ -463,13 +465,8 @@
             halves[c // half_width, part_rows, c % half_width : c % half_width + here] = (
                 gathered[part_rows, c : c + here] * inverse
             ).astype(jnp.bfloat16)
-        swap(i).start()
-    for i in range(2):
-        part_rows = slice(i * some, (i + 1) * some)
-        final[0, part_rows, :] = (
-            halves[core, part_rows, :].astype(jnp.float32) * gain
-        ).astype(jnp.bfloat16)
-        put(i, 0).start()
+        swap(i, core).start()
+        put(i).start()
 
     sent = pl.ds(0, Z * (X - 1) // X)
     remote(stage.at[sent], stage.at[sent], xsend.at[0], xrecv.at[0], ep=outward[0]).wait_send()
@@ -478,30 +475,22 @@
     for way in range(2):
         hop_sent(way, 1)
         remote(
-            ring.at[way], ring.at[way], bsend.at[way], brecv.at[way, 0], ep=homeward[way]
+            ring.at[way], ring.at[way], bsend.at[way], zrecv.at[way, 0], ep=homeward[way]
         ).wait_send()
     for i in range(2):
-        part_rows = slice(i * some, (i + 1) * some)
-        swap(i).wait_recv()
-        final[2, part_rows, :] = (
-            final[1, part_rows, :].astype(jnp.float32) * gain
-        ).astype(jnp.bfloat16)
-        put(i, 1).start()
-    for i in range(2):
-        swap(i).wait_send()
-        for who in range(2):
-            put(i, who).wait()
-
-
-def run_experts(plan, tokens, gain_in, expert_ids, gate_weights, w_gate, w_up, w_down, gain_out):
+        swap(i, core).wait_send()
+        swap(i, other).wait_recv()
+        put(i).wait()
+
+
+def run_experts(plan, tokens, gain_in, expert_ids, gate_weights, w_gate, w_up, w_down):
     X, Z, H, rows, width = plan.X, plan.Z, plan.H, plan.rows, plan.width
     dma = pltpu.SemaphoreType.DMA
-    hops = (2, sum(plan.pieces))
     bf16 = jnp.bfloat16
     return pl.pallas_call(
         functools.partial(experts_kernel, plan),
         out_shape=jax.ShapeDtypeStruct((2 * rows, width // 2), bf16),
-        in_specs=[VMEM, VMEM, VMEM, VMEM, ANY, ANY, ANY, VMEM],
+        in_specs=[VMEM, VMEM, VMEM, VMEM, ANY, ANY, ANY],
         out_specs=ANY,
         scratch_shapes=[
             pltpu.VMEM((rows, width), bf16),
@@ -520,13 +509,12 @@
             pltpu.VMEM((2,) + w_up.shape, bf16),
             pltpu.VMEM((2,) + w_down.shape, bf16),
             pltpu.VMEM((2, rows, width // 2), bf16),
-            pltpu.VMEM((3, rows, width // 2), bf16),
             pltpu.VMEM((2, rows, rows), bf16),
             pltpu.VMEM((2, rows, rows), bf16),
             pltpu.VMEM((rows, width), jnp.float32),
-            dma((2, H)), dma(hops), dma((2,)), dma(hops), dma((1,)), dma((2, H)),
+            dma((2, H)), dma((2, sum(plan.pieces) + plan.pieces[1])), dma((2,)), dma((1,)), dma((2, H)),
             dma((1,)), dma((Z,)), dma((1,)), dma((Z,)),
-            dma((3,)), dma((3,)), dma((3,)), dma((2,)), dma((2,)), dma((2, 2)),
+            dma((3,)), dma((3,)), dma((3,)), dma((2,)), dma((2,)), dma((2,)),
         ],
         compiler_params=pltpu.CompilerParams(
             collective_id=0, has_side_effects=True, vmem_limit_bytes=VMEM_LIMIT
@@ -534,8 +522,44 @@
         name="run_experts",
     )(
         tokens, gain_in.reshape(1, width), expert_ids.T, gate_weights.T,
-        w_gate, w_up, w_down, gain_out.reshape(1, width // 2),
+        w_gate, w_up, w_down,
     )
+
+
+CHUNKS = 4
+
+
+def gain_kernel(scaled_ref, gain_ref, out_ref, came, goes, in_sem, out_sem):
+    some = came.shape[1]
+
+    def load(i):
+        return pltpu.make_async_copy(scaled_ref.at[pl.ds(i * some, some), :], came.at[i], in_sem.at[i])
+
+    def store(i):
+        return pltpu.make_async_copy(goes.at[i], out_ref.at[pl.ds(i * some, some), :], out_sem.at[i])
+
+    for i in range(CHUNKS):
+        load(i).start()
+    for i in range(CHUNKS):
+        load(i).wait()
+        goes[i] = (came[i].astype(jnp.float32) * gain_ref[...]).astype(jnp.bfloat16)
+        store(i).start()
+    for i in range(CHUNKS):
+        store(i).wait()
+
+
+def apply_gain(scaled, gain_out):
+    rows, width = scaled.shape
+    part = pltpu.VMEM((CHUNKS, rows // CHUNKS, width), scaled.dtype)
+    dma = pltpu.SemaphoreType.DMA
+    return pl.pallas_call(
+        gain_kernel,
+        out_shape=jax.ShapeDtypeStruct(scaled.shape, scaled.dtype),
+        in_specs=[ANY, VMEM],
+        out_specs=ANY,
+        scratch_shapes=[part, part, dma((CHUNKS,)), dma((CHUNKS,))],
+        name="apply_gain",
+    )(scaled, gain_out.reshape(1, width))
 
 
 def per_device(columns, tokens, gain_in, expert_ids, gate_weights, w_gate, w_up, w_down, gain_out):
@@ -543,9 +567,10 @@
     members = lax.axis_size("ep")
     capacity = 2 * own_rows * expert_ids.shape[1] // members
     plan = Plan(own_rows, width, members, capacity, columns)
-    return run_experts(
-        plan, tokens, gain_in, expert_ids, gate_weights, w_gate[0], w_up[0], w_down[0], gain_out
+    scaled = run_experts(
+        plan, tokens, gain_in, expert_ids, gate_weights, w_gate[0], w_up[0], w_down[0]
     )
+    return apply_gain(scaled, gain_out)
 
 
 def solution(mesh, columns=COLUMNS):

time: 308 us -> 307 us (level)
  no operation moved by 1% of the time
where the time goes in v6:
time: 307 us
  Pallas kernels  307 us (100%)
    pallas_call x1, Pallas kernels, run_experts(): pl.pallas_call(functools.partial(experts_kernel, plan), out_shape=jax.Sha...  304 us

profile of v6, /device:TPU:33, one launch (start us, length us, event | category | flops | bytes accessed | tf_op | source)
XLA Modules:
  0.0 306.9 jit_solution(6240995520779374648)
XLA Ops:
  0.0 304.0 %run_experts.1.scaled_ref = bf16[512,1024]{1,0:T(8,128)(2,1)} custom-call(bf16[256,2048]{1,0:T(8,128)(2,1)} %x_ref.1, f32[1,2048]{1,0:T(1,128)} %bitcast.10, s32[2,512]{1,0:T(2,128)} %bitcast.11, f32[2,512]{1,0:T(2,128)} %bitcast.12, bf16[2048,256]{1,0:T(8,128)(2,1)} %bitcast.7, bf16[2048,256]{1,0:T(8,128)(2,1)} %bitcast.8, bf16[2048,256]{1,0:T(8,128)(2,1)} %bitcast.9), custom_call_target="tpu_custom_call" | custom-call | tf_op jit(solution)/shard_map/run_experts/pallas_call | solution.py:490
  304.0 2.7 apply_gain.1

commit v7 on v6

--- a/solution.py
+++ b/solution.py
@@ -62,20 +62,9 @@
     return lax.broadcasted_iota(jnp.int32, shape, dim)
 
 
-def sort_tokens(plan, x_ref, gain_ref, ids_ref, gates_ref, own, orders, meta_ref, normed):
+def sort_tokens(plan, loading, x_ref, gain_ref, ids_ref, gates_ref, own, orders, meta_ref, normed):
     rows, X, Z, H = plan.rows, plan.X, plan.Z, plan.H
     z, _ = plan.me()
-    step = 32
-
-    def norm_step(i, carry):
-        here = pl.ds(pl.multiple_of(i * step, step), step)
-        x = x_ref[here, :].astype(jnp.float32)
-        scale = lax.rsqrt(jnp.mean(x * x, axis=1, keepdims=True) + EPS)
-        normed[here, :] = (x * scale * gain_ref[...]).astype(jnp.bfloat16)
-        return carry
-
-    lax.fori_loop(0, rows // step, norm_step, 0)
-
     mine = pl.ds(pl.multiple_of(lax.axis_index("tp") * rows, rows), rows)
     square = (rows, rows)
     sub, lane = iota(square, 0), iota(square, 1)
@@ -123,6 +112,18 @@
         orders[way] = jnp.where(sub.astype(jnp.float32) == rank_row, 1.0, 0.0).astype(jnp.bfloat16)
     meta_ref[2, 6:8, :] = jnp.zeros((2, rows), jnp.float32)
 
+    loading.wait()
+    step = 32
+
+    def norm_step(i, carry):
+        here = pl.ds(pl.multiple_of(i * step, step), step)
+        x = x_ref[here, :].astype(jnp.float32)
+        scale = lax.rsqrt(jnp.mean(x * x, axis=1, keepdims=True) + EPS)
+        normed[here, :] = (x * scale * gain_ref[...]).astype(jnp.bfloat16)
+        return carry
+
+    lax.fori_loop(0, rows // step, norm_step, 0)
+
     def write(lo, hi):
         n = min(512, plan.width)
         for way in range(2):
@@ -181,10 +182,10 @@
     plan,
     x_ref, gain_ref, ids_ref, gates_ref, wg_ref, wu_ref, wd_ref,
     out_ref,
-    normed, plus_ref, minus_ref, meta_ref, ring, back, metas, stage, arrived, rows_in, spread, doubled,
+    tokens, normed, plus_ref, minus_ref, meta_ref, ring, back, metas, stage, arrived, rows_in, spread, doubled,
     wg, wu, wd, halves, orders, unsort, gathered,
     zsend, zrecv, bsend, msend, mrecv, xsend, xrecv, ysend, yrecv,
-    wsend, wrecv, wown, fsend, frecv, osem,
+    wsend, wrecv, wown, fsend, frecv, osem, tsem,
 ):
     X, Z, H, cap, piece = plan.X, plan.Z, plan.H, plan.cap, plan.piece
     rows, width, slots = plan.rows, plan.width, plan.slots
@@ -192,9 +193,13 @@
     z, x = plan.me()
     core = lax.axis_index("tp")
     other = 1 - core
+    loading = pltpu.make_async_copy(x_ref, tokens, tsem.at[0])
+    loading.start()
     barrier, peers = greet(plan)
     own = (plus_ref, minus_ref)
-    write = sort_tokens(plan, x_ref, gain_ref, ids_ref, gates_ref, own, orders, meta_ref, normed)
+    write = sort_tokens(
+        plan, loading, tokens, gain_ref, ids_ref, gates_ref, own, orders, meta_ref, normed
+    )
     lead = 3 * piece
     write(0, lead)
     pl.semaphore_wait(barrier, peers)
@@ -435,7 +440,8 @@
         gathered[:, c : c + wide] = part
     for way in range(2):
         closer(way, 1, plan.pieces[1] - 1).wait_recv()
-    half_width, some = width // 2, rows // 2
+    half_width, parts = width // 2, 4
+    some = rows // parts
     here = min(wide, half_width)
 
     def block(of, i):
@@ -448,7 +454,7 @@
     def put(i):
         return pltpu.make_async_copy(halves.at[core, pl.ds(i * some, some), :], block(core, i), osem.at[i])
 
-    for i in range(2):
+    for i in range(parts):
         part_rows = slice(i * some, (i + 1) * some)
         squares = jnp.zeros((some, 1), jnp.float32)
         for c in range(0, width, wide):
@@ -477,7 +483,7 @@
         remote(
             ring.at[way], ring.at[way], bsend.at[way], zrecv.at[way, 0], ep=homeward[way]
         ).wait_send()
-    for i in range(2):
+    for i in range(parts):
         swap(i, core).wait_send()
         swap(i, other).wait_recv()
         put(i).wait()
@@ -490,9 +496,10 @@
     return pl.pallas_call(
         functools.partial(experts_kernel, plan),
         out_shape=jax.ShapeDtypeStruct((2 * rows, width // 2), bf16),
-        in_specs=[VMEM, VMEM, VMEM, VMEM, ANY, ANY, ANY],
+        in_specs=[ANY, VMEM, VMEM, VMEM, ANY, ANY, ANY],
         out_specs=ANY,
         scratch_shapes=[
+            pltpu.VMEM((rows, width), bf16),
             pltpu.VMEM((rows, width), bf16),
             pltpu.VMEM((rows, width), bf16),
             pltpu.VMEM((rows, width), bf16),
@@ -514,7 +521,7 @@
             pltpu.VMEM((rows, width), jnp.float32),
             dma((2, H)), dma((2, sum(plan.pieces) + plan.pieces[1])), dma((2,)), dma((1,)), dma((2, H)),
             dma((1,)), dma((Z,)), dma((1,)), dma((Z,)),
-            dma((3,)), dma((3,)), dma((3,)), dma((2,)), dma((2,)), dma((2,)),
+            dma((3,)), dma((3,)), dma((3,)), dma((4,)), dma((4,)), dma((4,)), dma((1,)),
         ],
         compiler_params=pltpu.CompilerParams(
             collective_id=0, has_side_effects=True, vmem_limit_bytes=VMEM_LIMIT
@@ -526,42 +533,6 @@
     )
 
 
-CHUNKS = 4
-
-
-def gain_kernel(scaled_ref, gain_ref, out_ref, came, goes, in_sem, out_sem):
-    some = came.shape[1]
-
-    def load(i):
-        return pltpu.make_async_copy(scaled_ref.at[pl.ds(i * some, some), :], came.at[i], in_sem.at[i])
-
-    def store(i):
-        return pltpu.make_async_copy(goes.at[i], out_ref.at[pl.ds(i * some, some), :], out_sem.at[i])
-
-    for i in range(CHUNKS):
-        load(i).start()
-    for i in range(CHUNKS):
-        load(i).wait()
-        goes[i] = (came[i].astype(jnp.float32) * gain_ref[...]).astype(jnp.bfloat16)
-        store(i).start()
-    for i in range(CHUNKS):
-        store(i).wait()
-
-
-def apply_gain(scaled, gain_out):
-    rows, width = scaled.shape
-    part = pltpu.VMEM((CHUNKS, rows // CHUNKS, width), scaled.dtype)
-    dma = pltpu.SemaphoreType.DMA
-    return pl.pallas_call(
-        gain_kernel,
-        out_shape=jax.ShapeDtypeStruct(scaled.shape, scaled.dtype),
-        in_specs=[ANY, VMEM],
-        out_specs=ANY,
-        scratch_shapes=[part, part, dma((CHUNKS,)), dma((CHUNKS,))],
-        name="apply_gain",
-    )(scaled, gain_out.reshape(1, width))
-
-
 def per_device(columns, tokens, gain_in, expert_ids, gate_weights, w_gate, w_up, w_down, gain_out):
     own_rows, width = tokens.shape
     members = lax.axis_size("ep")
@@ -570,7 +541,7 @@
     scaled = run_experts(
         plan, tokens, gain_in, expert_ids, gate_weights, w_gate[0], w_up[0], w_down[0]
     )
-    return apply_gain(scaled, gain_out)
+    return (scaled.astype(jnp.float32) * gain_out).astype(jnp.bfloat16)
 
 
 def solution(mesh, columns=COLUMNS):

time: 307 us -> 307 us (level)
  no operation moved by 1% of the time
where the time goes in v7:
time: 307 us; the launch traced here: 306 us
  Pallas kernels  304 us (99%)
    pallas_call x1, Pallas kernels, run_experts(): pl.pallas_call(functools.partial(experts_kernel, plan), out_shape=jax.Sha...  304 us

profile of v7, /device:TPU:33, one launch (start us, length us, event | category | flops | bytes accessed | tf_op | source)
XLA Modules:
  0.0 306.4 jit_solution(15824572094504658245)
XLA Ops:
  0.0 0.0 copy-start
  0.0 303.9 %run_experts.1 = bf16[512,1024]{1,0:T(8,128)(2,1)} custom-call(bf16[256,2048]{1,0:T(8,128)(2,1)} %x_ref.1, f32[1,2048]{1,0:T(1,128)} %bitcast.9, s32[2,512]{1,0:T(2,128)} %bitcast.10, f32[2,512]{1,0:T(2,128)} %bitcast.11, bf16[2048,256]{1,0:T(8,128)(2,1)} %bitcast.6, bf16[2048,256]{1,0:T(8,128)(2,1)} %bitcast.7, bf16[2048,256]{1,0:T(8,128)(2,1)} %bitcast.8), custom_call_target="tpu_custom_call" | custom-call | tf_op jit(solution)/shard_map/run_experts/pallas_call | solution.py:496
  303.9 0.0 copy-done
  303.9 2.4 multiply_convert_fusion
Async XLA Ops:
  0.0 303.9 %copy-start = (f32[1024]{0:T(1024)S(1)}, f32[1024]{0:T(1024)}, u32[]{:S(2)}) copy-start(f32[1024]{0:T(1024)} %param.15) | copy-start | bytes 12292
